TPU v7x, 512 devices: a whole 4x4x16 slice. The times are simulated.
512 devices in a mesh: kv: 64 (over z, y), tp: 8 (over x, core).
Axes of the slice: x: 4, y: 4, z: 16, core: 2. Of those that a mesh axis runs over, the one named last changes fastest.
Arguments:
- tokens: bfloat16 [256, 2048], P('tp', 'kv'), may hold values from -24 to 24
- lengths: int32 [64], P('kv'), may hold values from 1 to 4, 160 in all
- memory_state: float32 [64, 16, 128, 128], P('kv', 'tp'), may hold values from -3 to 3
- gain_first: float32 [2048], P('kv'), may hold values from 0.1 to 1.9
- first_gate: bfloat16 [2048, 5120], P('kv', 'tp'), may hold values from -0.125 to 0.125
- first_up: bfloat16 [2048, 5120], P('kv', 'tp'), may hold values from -0.125 to 0.125
- first_down: bfloat16 [5120, 2048], P('tp', 'kv'), may hold values from -0.15625 to 0.15625
- gain_mixer: float32 [2048], P('kv'), may hold values from 0.1 to 1.9
- query_weight: bfloat16 [2048, 2048], P('kv', 'tp'), may hold values from -0.125 to 0.125
- key_weight: bfloat16 [2048, 2048], P('kv', 'tp'), may hold values from -0.125 to 0.125
- value_weight: bfloat16 [2048, 2048], P('kv', 'tp'), may hold values from -0.125 to 0.125
- outgate_weight: bfloat16 [2048, 2048], P('kv', 'tp'), may hold values from -0.125 to 0.125
- beta_weight: bfloat16 [2048, 16], P('kv'), may hold values from -0.125 to 0.125
- decay_weight: bfloat16 [2048, 16], P('kv'), may hold values from -0.125 to 0.125
- decay_rate: float32 [16], P('tp'), may hold values from 0.05 to 4
- decay_bias: float32 [16], P('tp'), may hold values from -3 to 1
- head_gain: float32 [128], replicated, may hold values from 0.1 to 1.9
- out_weight: bfloat16 [2048, 2048], P('tp', 'kv'), may hold values from -0.25 to 0.25
- gain_second: float32 [2048], P('kv'), may hold values from 0.1 to 1.9
- second_gate: bfloat16 [2048, 5120], P('kv', 'tp'), may hold values from -0.125 to 0.125
- second_up: bfloat16 [2048, 5120], P('kv', 'tp'), may hold values from -0.125 to 0.125
- second_down: bfloat16 [5120, 2048], P('tp', 'kv'), may hold values from -0.15625 to 0.15625
Outputs:
- layer_out: bfloat16 [256, 2048], P('tp', 'kv')
- state_out: float32 [64, 16, 128, 128], P('kv', 'tp')
Inputs may be any that keep to these rules, and one draw needn't show every extreme that they name: `lengths`: each sequence's count of live new token slots.
All inputs are finite; a program needn't handle non-finite values. No bound on the sum of `lengths` on one device may be relied on, other than what follows from the above.
Results may differ from a plain program's by a relative error of at most 0.02.
Values may be sent and summed in bfloat16 or wider, within the bound.
No kernel may reach another device: no remote copies, remote signals or barrier semaphores. Data moves between devices by JAX's collectives and lax.ppermute only.
A program may use at most 64 MiB of HBM per device.

v0:
```python
import jax
import jax.numpy as jnp
from jax import lax
from jax.sharding import PartitionSpec as P

D = 2048
HEAD_DIM = 128
NEW = 4


EPS = 1e-06


def from_everyone(x, axis):
    count = lax.axis_size(axis)
    return lax.all_to_all(jnp.broadcast_to(x[None], (count, *x.shape)), axis, 0, 0, tiled=True)


def laid_out(pieces, dim):
    dims = list(pieces.shape[1:])
    dims[dim] *= pieces.shape[0]
    return jnp.moveaxis(pieces, 0, dim).reshape(dims)


def gather_directly(x, axis, dim):
    pieces = from_everyone(x, axis)
    return laid_out(pieces, dim)


def cut_along(x, dim, count):
    dims = x.shape
    pieces = x.reshape(*dims[:dim], count, dims[dim] // count, *dims[dim + 1 :])
    return jnp.moveaxis(pieces, dim, 0)


def sent_and_summed(x, axis, dim):
    count = lax.axis_size(axis)
    pieces = lax.all_to_all(cut_along(x, dim, count), axis, 0, 0, tiled=True)
    return jnp.sum(pieces.astype(jnp.float32), axis=0)


def in_one_piece(arrays, axis, dim, along):
    columns = [a.reshape(*a.shape[:along], -1) for a in arrays]
    both = jnp.concatenate(columns, axis=along)
    result, at, finished = (sent_and_summed(both, axis, dim), 0, [])
    for a, column in zip(arrays, columns):
        slab = result[..., at : at + column.shape[along]]
        finished.append(slab.reshape(*slab.shape[:along], *a.shape[along:]))
        at += column.shape[along]
    return tuple(finished)


def normed_operand(resid, gain):
    widened = resid.astype(jnp.float32)
    squares = jnp.sum(widened * widened, axis=1)
    operand = (widened * gain).astype(jnp.bfloat16)
    return (operand, squares)


def inverse_rms(squares):
    return lax.rsqrt(squares / D + EPS)[:, None]


def gather_rows(resid, gain):
    operand, squares = normed_operand(resid, gain)
    gathered, gathered_squares = (
        gather_directly(operand, "tp", 0),
        gather_directly(squares.astype(jnp.bfloat16), "tp", 0).astype(squares.dtype),
    )
    return (gathered, gathered_squares)


def advance(
    query_part,
    key_part,
    value_part,
    outgate_part,
    beta_logit,
    decay_logit,
    state_now,
    lengths,
    decay_rate,
    decay_bias,
    head_gain,
):
    seqs = state_now.shape[0]
    heads = state_now.shape[1]

    def split_heads(matrix):
        return matrix.reshape(seqs, NEW, heads, HEAD_DIM)

    query = split_heads(jax.nn.silu(query_part))
    query = (
        query * lax.rsqrt(jnp.sum(query * query, axis=-1, keepdims=True) + EPS) * HEAD_DIM ** (-0.5)
    )
    keyvec = split_heads(jax.nn.silu(key_part))
    keyvec = keyvec * lax.rsqrt(jnp.sum(keyvec * keyvec, axis=-1, keepdims=True) + EPS)
    values = split_heads(jax.nn.silu(value_part))
    live_mask = (jnp.arange(NEW, dtype=jnp.int32)[None, :] < lengths[:, None]).astype(jnp.float32)[
        :, :, None
    ]
    beta_gate = jax.nn.sigmoid(beta_logit.reshape(seqs, NEW, heads)) * live_mask
    decay_log = (
        -decay_rate
        * jax.nn.softplus(decay_logit.reshape(seqs, NEW, heads) + decay_bias)
        * live_mask
    )
    outputs = []
    for position in range(NEW):
        state_now = state_now * jnp.exp(decay_log[:, position])[:, :, None, None]
        predicted = jnp.einsum(
            "shk,shkv->shv", keyvec[:, position], state_now, precision=lax.Precision.HIGHEST
        )
        update = beta_gate[:, position][:, :, None] * (values[:, position] - predicted)
        state_now = state_now + keyvec[:, position][:, :, :, None] * update[:, :, None, :]
        outputs.append(
            jnp.einsum(
                "shk,shkv->shv", query[:, position], state_now, precision=lax.Precision.HIGHEST
            )
        )
    mixed = jnp.stack(outputs, axis=1) * live_mask[..., None]
    mixed = mixed * lax.rsqrt(jnp.mean(mixed * mixed, axis=-1, keepdims=True) + EPS) * head_gain
    mixed = mixed * jax.nn.silu(split_heads(outgate_part))
    return (mixed.reshape(seqs * NEW, heads * HEAD_DIM).astype(jnp.bfloat16), state_now)


def channel_mix(resid, gain, w_gate, w_up, w_down):
    gathered, squares = gather_rows(resid, gain)
    gate_part = jnp.dot(gathered, w_gate, preferred_element_type=jnp.float32)
    up_part = jnp.dot(gathered, w_up, preferred_element_type=jnp.float32)
    gate_part, up_part, squares = in_one_piece(
        (
            gate_part.astype(jnp.bfloat16),
            up_part.astype(jnp.bfloat16),
            squares.astype(jnp.bfloat16),
        ),
        "kv",
        0,
        1,
    )
    scale = inverse_rms(squares)
    hidden = (jax.nn.silu(gate_part * scale) * (up_part * scale)).astype(jnp.bfloat16)
    hidden = gather_directly(hidden, "kv", 0)
    branch = sent_and_summed(
        jnp.dot(hidden, w_down, preferred_element_type=jnp.float32).astype(jnp.bfloat16), "tp", 0
    )
    return (resid.astype(jnp.float32) + 0.5 * branch).astype(jnp.bfloat16)


def token_mix(
    resid,
    gain,
    query_weight,
    key_weight,
    value_weight,
    outgate_weight,
    beta_weight,
    decay_weight,
    memory_state,
    lengths,
    decay_rate,
    decay_bias,
    head_gain,
    out_weight,
):
    gathered, squares = gather_rows(resid, gain)

    def project(weight):
        return jnp.dot(gathered, weight, preferred_element_type=jnp.float32)

    query_sum = project(query_weight)
    key_sum = project(key_weight)
    value_sum = project(value_weight)
    outgate_sum = project(outgate_weight)
    beta_sum = project(beta_weight)
    decay_sum = project(decay_weight)
    query_sum, key_sum, value_sum, outgate_sum, beta_sum, decay_sum, squares = in_one_piece(
        (
            query_sum.astype(jnp.bfloat16),
            key_sum.astype(jnp.bfloat16),
            value_sum.astype(jnp.bfloat16),
            outgate_sum.astype(jnp.bfloat16),
            beta_sum.astype(jnp.bfloat16),
            decay_sum.astype(jnp.bfloat16),
            squares.astype(jnp.bfloat16),
        ),
        "kv",
        0,
        1,
    )
    scale = inverse_rms(squares)
    head_count = memory_state.shape[1]
    first_head = lax.axis_index("tp") * head_count
    beta_logit = lax.dynamic_slice_in_dim(beta_sum * scale, first_head, head_count, 1)
    decay_logit = lax.dynamic_slice_in_dim(decay_sum * scale, first_head, head_count, 1)
    mixed, state_out = advance(
        query_sum * scale,
        key_sum * scale,
        value_sum * scale,
        outgate_sum * scale,
        beta_logit,
        decay_logit,
        memory_state,
        lengths,
        decay_rate,
        decay_bias,
        head_gain,
    )
    all_heads = gather_directly(mixed, "kv", 0)
    branch = sent_and_summed(
        jnp.dot(all_heads, out_weight, preferred_element_type=jnp.float32).astype(jnp.bfloat16),
        "tp",
        0,
    )
    return ((resid.astype(jnp.float32) + branch).astype(jnp.bfloat16), state_out)


def on_device(
    tokens,
    lengths,
    memory_state,
    gain_first,
    first_gate,
    first_up,
    first_down,
    gain_mixer,
    query_weight,
    key_weight,
    value_weight,
    outgate_weight,
    beta_weight,
    decay_weight,
    decay_rate,
    decay_bias,
    head_gain,
    out_weight,
    gain_second,
    second_gate,
    second_up,
    second_down,
):
    first = channel_mix(tokens, gain_first, first_gate, first_up, first_down)
    second, state_out = token_mix(
        first,
        gain_mixer,
        query_weight,
        key_weight,
        value_weight,
        outgate_weight,
        beta_weight,
        decay_weight,
        memory_state,
        lengths,
        decay_rate,
        decay_bias,
        head_gain,
        out_weight,
    )
    layer_out = channel_mix(second, gain_second, second_gate, second_up, second_down)
    return (layer_out, state_out)


def solution(mesh):
    in_specs = (
        P("tp", "kv"),
        P("kv"),
        P("kv", "tp", None, None),
        P("kv"),
        P("kv", "tp"),
        P("kv", "tp"),
        P("tp", "kv"),
        P("kv"),
        P("kv", "tp"),
        P("kv", "tp"),
        P("kv", "tp"),
        P("kv", "tp"),
        P("kv", None),
        P("kv", None),
        P("tp"),
        P("tp"),
        P(),
        P("tp", "kv"),
        P("kv"),
        P("kv", "tp"),
        P("kv", "tp"),
        P("tp", "kv"),
    )
    out_specs = (P("tp", "kv"), P("kv", "tp", None, None))
    return jax.shard_map(
        on_device, mesh=mesh, in_specs=in_specs, out_specs=out_specs, check_vma=False
    )
```

profile of v0, /device:TPU:1, one launch (start us, length us, event | category | flops | bytes accessed | tf_op | source)
XLA Modules:
  0.0 325.1 jit_solution(103894445208054434)
XLA Ops:
  0.6 0.8 copy.50
  1.4 0.7 fusion.36
  2.2 0.6 broadcast_in_dim.19
  2.8 10.1 %all-to-all-start.1 = ((bf16[8,1,32]{2,1,0:T(2,128)(2,1)}), bf16[8,1,32]{2,1,0:T(2,128)(2,1)S(1)}, u32[]{:S(2)}, u32[]{:S(2)}) async-start(bf16[8,1,32]{2,1,0:T(2,128)(2,1)} %broadcast_in_dim.19), calls=%async_computation.1 | async-start | bytes 8192 | tf_op jit(solution)/shard_map/all_to_all | solution.py:16
  12.9 0.7 reshape.574
  13.6 3.7 %all-to-all-done.1 = bf16[8,1,32]{2,1,0:T(2,128)(2,1)S(1)} async-done(((bf16[8,1,32]{2,1,0:T(2,128)(2,1)}), bf16[8,1,32]{2,1,0:T(2,128)(2,1)S(1)}, u32[]{:S(2)}, u32[]{:S(2)}) %all-to-all-start.1) | async-done | bytes 544 | tf_op jit(solution)/shard_map/all_to_all | solution.py:16
  17.4 3.9 %all-to-all-start = ((bf16[8,2,512]{2,1,0:T(2,128)(2,1)}), bf16[8,2,512]{2,1,0:T(2,128)(2,1)S(1)}, u32[]{:S(2)}, u32[]{:S(2)}) async-start(bf16[8,2,512]{2,1,0:T(2,128)(2,1)} %reshape.574), calls=%async_computation | async-start | bytes 32768 | tf_op jit(solution)/shard_map/all_to_all | solution.py:16
  21.3 0.2 concatenate.64
  21.5 4.5 %all-to-all-done = bf16[8,2,512]{2,1,0:T(2,128)(2,1)S(1)} async-done(((bf16[8,2,512]{2,1,0:T(2,128)(2,1)}), bf16[8,2,512]{2,1,0:T(2,128)(2,1)S(1)}, u32[]{:S(2)}, u32[]{:S(2)}) %all-to-all-start) | async-done | bytes 16416 | tf_op jit(solution)/shard_map/all_to_all | solution.py:16
  26.1 0.2 convolution_convert_fusion.2
  26.4 0.2 convolution_convert_fusion.3
  26.7 0.3 pad_maximum_fusion
  27.0 52.0 %all_to_all.78 = bf16[64,4,1281]{2,1,0:T(4,128)(2,1)S(1)} all-to-all(bf16[64,4,1281]{2,1,0:T(4,128)(2,1)S(1)} %pad_maximum_fusion), channel_id=1, replica_groups=mesh['kv'=64,'tp'=8] {'kv'}, dimensions={0} | all-to-all | bytes 1311744 | tf_op jit(solution)/shard_map/all_to_all | solution.py:38
  79.1 0.3 convert_reduce_fusion.1
  79.7 29.8 %all_to_all.79 = bf16[64,4,640]{2,1,0:T(4,128)(2,1)S(1)} all-to-all(bf16[64,4,640]{2,1,0:T(4,128)(2,1)S(1)} %broadcast_in_dim.20), channel_id=1, replica_groups=mesh['kv'=64,'tp'=8] {'kv'}, dimensions={0} | all-to-all | bytes 655360 | tf_op jit(solution)/shard_map/all_to_all | solution.py:16
  109.7 0.2 convolution_convert_fusion.10
  109.8 0.2 reshape.522
  110.1 11.8 %all_to_all.80 = bf16[8,2,512]{2,1,0:T(2,128)(2,1)S(1)} all-to-all(bf16[8,2,512]{2,1,0:T(2,128)(2,1)S(1)} %reshape.576), channel_id=1, replica_groups=mesh['kv'=64,'tp'=8] {'tp'}, dimensions={0} | all-to-all | bytes 32768 | tf_op jit(solution)/shard_map/all_to_all | solution.py:38
  122.1 0.6 broadcast_in_dim.22
  122.7 3.9 %all-to-all-start.6 = ((bf16[8,1,32]{2,1,0:T(2,128)(2,1)}), bf16[8,1,32]{2,1,0:T(2,128)(2,1)S(1)}, u32[]{:S(2)}, u32[]{:S(2)}) async-start(bf16[8,1,32]{2,1,0:T(2,128)(2,1)} %broadcast_in_dim.22), calls=%async_computation.6 | async-start | bytes 8192 | tf_op jit(solution)/shard_map/all_to_all | solution.py:16
  126.8 0.7 reshape.578
  127.5 3.6 %all-to-all-done.6 = bf16[8,1,32]{2,1,0:T(2,128)(2,1)S(1)} async-done(((bf16[8,1,32]{2,1,0:T(2,128)(2,1)}), bf16[8,1,32]{2,1,0:T(2,128)(2,1)S(1)}, u32[]{:S(2)}, u32[]{:S(2)}) %all-to-all-start.6) | async-done | bytes 544 | tf_op jit(solution)/shard_map/all_to_all | solution.py:16
  131.1 3.9 %all-to-all-start.5 = ((bf16[8,2,512]{2,1,0:T(2,128)(2,1)}), bf16[8,2,512]{2,1,0:T(2,128)(2,1)S(1)}, u32[]{:S(2)}, u32[]{:S(2)}) async-start(bf16[8,2,512]{2,1,0:T(2,128)(2,1)} %reshape.578), calls=%async_computation.5 | async-start | bytes 32768 | tf_op jit(solution)/shard_map/all_to_all | solution.py:16
  135.1 0.2 concatenate.65
  135.3 4.5 %all-to-all-done.5 = bf16[8,2,512]{2,1,0:T(2,128)(2,1)S(1)} async-done(((bf16[8,2,512]{2,1,0:T(2,128)(2,1)}), bf16[8,2,512]{2,1,0:T(2,128)(2,1)S(1)}, u32[]{:S(2)}, u32[]{:S(2)}) %all-to-all-start.5) | async-done | bytes 16416 | tf_op jit(solution)/shard_map/all_to_all | solution.py:16
  140.4 0.2 convolution_convert_fusion.4
  140.7 0.2 convolution_convert_fusion.5
  140.9 0.2 convolution_convert_fusion.6
  141.4 2.5 concatenate.59
  143.9 4.8 %all-to-all-start.7 = ((bf16[64,4,1057]{2,1,0:T(4,128)(2,1)}), bf16[64,4,1057]{2,1,0:T(4,128)(2,1)S(1)}, u32[]{:S(2)}, u32[]{:S(2)}) async-start(bf16[64,4,1057]{2,1,0:T(4,128)(2,1)} %concatenate.59), calls=%async_computation.7 | async-start | bytes 1179648 | tf_op jit(solution)/shard_map/all_to_all | solution.py:38
  149.4 32.5 %all-to-all-done.7 = bf16[64,4,1057]{2,1,0:T(4,128)(2,1)S(1)} async-done(((bf16[64,4,1057]{2,1,0:T(4,128)(2,1)}), bf16[64,4,1057]{2,1,0:T(4,128)(2,1)S(1)}, u32[]{:S(2)}, u32[]{:S(2)}) %all-to-all-start.7) | async-done | bytes 541216 | tf_op jit(solution)/shard_map/all_to_all | solution.py:38
  181.9 0.3 convert_reduce_fusion.2
  182.2 0.2 fusion.61
  182.8 0.2 exponential_reduce_fusion.1
  183.1 0.2 slice_reduce_fusion
  183.7 0.3 fusion.14
  184.1 0.3 fusion.12
  184.4 0.3 fusion.10
  184.9 0.2 fusion.8
  185.1 0.3 fusion.6
  185.5 0.3 fusion.4
  185.8 0.3 fusion.2
  186.2 0.2 multiply_add_fusion
  186.5 0.2 fusion
  186.7 0.2 fusion.52
  187.1 22.3 %all_to_all.81 = bf16[64,4,256]{2,1,0:T(4,128)(2,1)S(1)} all-to-all(bf16[64,4,256]{2,1,0:T(4,128)(2,1)S(1)} %broadcast_in_dim.23), channel_id=1, replica_groups=mesh['kv'=64,'tp'=8] {'kv'}, dimensions={0} | all-to-all | bytes 262144 | tf_op jit(solution)/shard_map/all_to_all | solution.py:16
  209.8 10.6 %all_to_all.82 = bf16[8,2,512]{2,1,0:T(2,128)(2,1)S(1)} all-to-all(bf16[8,2,512]{2,1,0:T(2,128)(2,1)S(1)} %reshape.580), channel_id=1, replica_groups=mesh['kv'=64,'tp'=8] {'tp'}, dimensions={0} | all-to-all | bytes 32768 | tf_op jit(solution)/shard_map/all_to_all | solution.py:38
  220.7 0.6 broadcast_in_dim.25
  221.3 3.9 %all-to-all-start.11 = ((bf16[8,1,32]{2,1,0:T(2,128)(2,1)}), bf16[8,1,32]{2,1,0:T(2,128)(2,1)S(1)}, u32[]{:S(2)}, u32[]{:S(2)}) async-start(bf16[8,1,32]{2,1,0:T(2,128)(2,1)} %broadcast_in_dim.25), calls=%async_computation.11 | async-start | bytes 8192 | tf_op jit(solution)/shard_map/all_to_all | solution.py:16
  225.3 0.7 reshape.582
  226.0 3.7 %all-to-all-done.11 = bf16[8,1,32]{2,1,0:T(2,128)(2,1)S(1)} async-done(((bf16[8,1,32]{2,1,0:T(2,128)(2,1)}), bf16[8,1,32]{2,1,0:T(2,128)(2,1)S(1)}, u32[]{:S(2)}, u32[]{:S(2)}) %all-to-all-start.11) | async-done | bytes 544 | tf_op jit(solution)/shard_map/all_to_all | solution.py:16
  229.8 3.9 %all-to-all-start.10 = ((bf16[8,2,512]{2,1,0:T(2,128)(2,1)}), bf16[8,2,512]{2,1,0:T(2,128)(2,1)S(1)}, u32[]{:S(2)}, u32[]{:S(2)}) async-start(bf16[8,2,512]{2,1,0:T(2,128)(2,1)} %reshape.582), calls=%async_computation.10 | async-start | bytes 32768 | tf_op jit(solution)/shard_map/all_to_all | solution.py:16
  233.7 0.2 concatenate.66
  233.9 4.5 %all-to-all-done.10 = bf16[8,2,512]{2,1,0:T(2,128)(2,1)S(1)} async-done(((bf16[8,2,512]{2,1,0:T(2,128)(2,1)}), bf16[8,2,512]{2,1,0:T(2,128)(2,1)S(1)}, u32[]{:S(2)}, u32[]{:S(2)}) %all-to-all-start.10) | async-done | bytes 16416 | tf_op jit(solution)/shard_map/all_to_all | solution.py:16
  238.5 0.2 convolution_convert_fusion
  238.8 0.2 convolution_convert_fusion.1
  239.1 0.3 pad_maximum_fusion.1
  239.5 42.3 %all_to_all.83 = bf16[64,4,1281]{2,1,0:T(4,128)(2,1)S(1)} all-to-all(bf16[64,4,1281]{2,1,0:T(4,128)(2,1)S(1)} %pad_maximum_fusion.1), channel_id=1, replica_groups=mesh['kv'=64,'tp'=8] {'kv'}, dimensions={0} | all-to-all | bytes 1311744 | tf_op jit(solution)/shard_map/all_to_all | solution.py:38
  281.7 0.3 convert_reduce_fusion
  282.4 29.6 %all_to_all.84 = bf16[64,4,640]{2,1,0:T(4,128)(2,1)S(1)} all-to-all(bf16[64,4,640]{2,1,0:T(4,128)(2,1)S(1)} %broadcast_in_dim.26), channel_id=1, replica_groups=mesh['kv'=64,'tp'=8] {'kv'}, dimensions={0} | all-to-all | bytes 655360 | tf_op jit(solution)/shard_map/all_to_all | solution.py:16
  312.0 0.2 convolution_convert_fusion.9
  312.2 0.2 reshape.543
  312.5 11.8 %all_to_all.85 = bf16[8,2,512]{2,1,0:T(2,128)(2,1)S(1)} all-to-all(bf16[8,2,512]{2,1,0:T(2,128)(2,1)S(1)} %reshape.584), channel_id=1, replica_groups=mesh['kv'=64,'tp'=8] {'tp'}, dimensions={0} | all-to-all | bytes 32768 | tf_op jit(solution)/shard_map/all_to_all | solution.py:38
  324.4 0.7 copy.67
  (121 shorter events, 5.5 us)
Async XLA Ops:
  0.6 25.4 %copy-start = (bf16[32,640]{1,0:T(8,128)(2,1)S(1)}, bf16[32,640]{1,0:T(8,128)(2,1)}, u32[]{:S(2)}) copy-start(bf16[32,640]{1,0:T(8,128)(2,1)} %param.27) | copy-start | bytes 122884
  2.8 14.6 %all-to-all-start.1 = ((bf16[8,1,32]{2,1,0:T(2,128)(2,1)}), bf16[8,1,32]{2,1,0:T(2,128)(2,1)S(1)}, u32[]{:S(2)}, u32[]{:S(2)}) async-start(bf16[8,1,32]{2,1,0:T(2,128)(2,1)} %broadcast_in_dim.19), calls=%async_computation.1 | async-start | bytes 8192 | tf_op jit(solution)/shard_map/all_to_all | solution.py:16
  12.9 13.5 %copy-start.5 = (bf16[32,640]{1,0:T(8,128)(2,1)S(1)}, bf16[32,640]{1,0:T(8,128)(2,1)}, u32[]{:S(2)}) copy-start(bf16[32,640]{1,0:T(8,128)(2,1)} %param.26) | copy-start | bytes 122884
  17.4 8.6 %all-to-all-start = ((bf16[8,2,512]{2,1,0:T(2,128)(2,1)}), bf16[8,2,512]{2,1,0:T(2,128)(2,1)S(1)}, u32[]{:S(2)}, u32[]{:S(2)}) async-start(bf16[8,2,512]{2,1,0:T(2,128)(2,1)} %reshape.574), calls=%async_computation | async-start | bytes 32768 | tf_op jit(solution)/shard_map/all_to_all | solution.py:16
  79.7 29.9 %copy-start.3 = (bf16[640,32]{0,1:T(8,128)(2,1)S(1)}, bf16[640,32]{0,1:T(8,128)(2,1)}, u32[]{:S(2)}) copy-start(bf16[640,32]{0,1:T(8,128)(2,1)} %param.28) | copy-start | bytes 122884
  109.5 17.1 %copy-start.15 = (f32[32]{0:T(128)S(1)}, f32[32]{0:T(128)}, u32[]{:S(2)}) copy-start(f32[32]{0:T(128)} %param.29) | copy-start | bytes 388
  109.6 30.2 %copy-start.13 = (bf16[32,16]{0,1:T(8,128)(2,1)S(1)}, bf16[32,16]{0,1:T(8,128)(2,1)}, u32[]{:S(2)}) copy-start(bf16[32,16]{0,1:T(8,128)(2,1)} %param.35) | copy-start | bytes 3076
  109.6 30.4 %copy-start.14 = (bf16[32,16]{0,1:T(8,128)(2,1)S(1)}, bf16[32,16]{0,1:T(8,128)(2,1)}, u32[]{:S(2)}) copy-start(bf16[32,16]{0,1:T(8,128)(2,1)} %param.34) | copy-start | bytes 3076
  109.6 30.8 %copy-start.9 = (bf16[32,256]{1,0:T(8,128)(2,1)S(1)}, bf16[32,256]{1,0:T(8,128)(2,1)}, u32[]{:S(2)}) copy-start(bf16[32,256]{1,0:T(8,128)(2,1)} %param.33) | copy-start | bytes 49156
  110.1 30.5 %copy-start.10 = (bf16[32,256]{1,0:T(8,128)(2,1)S(1)}, bf16[32,256]{1,0:T(8,128)(2,1)}, u32[]{:S(2)}) copy-start(bf16[32,256]{1,0:T(8,128)(2,1)} %param.32) | copy-start | bytes 49156
  122.7 8.5 %all-to-all-start.6 = ((bf16[8,1,32]{2,1,0:T(2,128)(2,1)}), bf16[8,1,32]{2,1,0:T(2,128)(2,1)S(1)}, u32[]{:S(2)}, u32[]{:S(2)}) async-start(bf16[8,1,32]{2,1,0:T(2,128)(2,1)} %broadcast_in_dim.22), calls=%async_computation.6 | async-start | bytes 8192 | tf_op jit(solution)/shard_map/all_to_all | solution.py:16
  127.5 13.4 %copy-start.11 = (bf16[32,256]{1,0:T(8,128)(2,1)S(1)}, bf16[32,256]{1,0:T(8,128)(2,1)}, u32[]{:S(2)}) copy-start(bf16[32,256]{1,0:T(8,128)(2,1)} %param.31) | copy-start | bytes 49156
  131.1 8.6 %all-to-all-start.5 = ((bf16[8,2,512]{2,1,0:T(2,128)(2,1)}), bf16[8,2,512]{2,1,0:T(2,128)(2,1)S(1)}, u32[]{:S(2)}, u32[]{:S(2)}) async-start(bf16[8,2,512]{2,1,0:T(2,128)(2,1)} %reshape.578), calls=%async_computation.5 | async-start | bytes 32768 | tf_op jit(solution)/shard_map/all_to_all | solution.py:16
  140.4 0.7 copy-start.12
  143.9 5.5 %copy-start.18 = (f32[2]{0:T(128)S(1)}, f32[2]{0:T(128)}, u32[]{:S(2)}) copy-start(f32[2]{0:T(128)} %param.36) | copy-start | bytes 28
  143.9 5.5 %copy-start.19 = (f32[128]{0:T(128)S(1)}, f32[128]{0:T(128)}, u32[]{:S(2)}) copy-start(f32[128]{0:T(128)} %param.38) | copy-start | bytes 1540
  143.9 38.6 %copy-start.16 = (f32[2]{0:T(128)S(1)}, f32[2]{0:T(128)}, u32[]{:S(2)}) copy-start(f32[2]{0:T(128)} %param.37) | copy-start | bytes 28
  143.9 39.8 %copy-start.1 = (f32[1,2,128,128]{3,2,1,0:T(8,128)S(1)}, f32[1,2,128,128]{3,2,1,0:T(8,128)}, u32[]{:S(2)}) copy-start(f32[1,2,128,128]{3,2,1,0:T(8,128)} %param.24) | copy-start | bytes 393220
  143.9 38.0 %all-to-all-start.7 = ((bf16[64,4,1057]{2,1,0:T(4,128)(2,1)}), bf16[64,4,1057]{2,1,0:T(4,128)(2,1)S(1)}, u32[]{:S(2)}, u32[]{:S(2)}) async-start(bf16[64,4,1057]{2,1,0:T(4,128)(2,1)} %concatenate.59), calls=%async_computation.7 | async-start | bytes 1179648 | tf_op jit(solution)/shard_map/all_to_all | solution.py:38
  185.5 23.9 %copy-start.8 = (bf16[256,32]{0,1:T(8,128)(2,1)S(1)}, bf16[256,32]{0,1:T(8,128)(2,1)}, u32[]{:S(2)}) copy-start(bf16[256,32]{0,1:T(8,128)(2,1)} %param.39) | copy-start | bytes 49156
  186.4 34.1 %copy-start.2 = (f32[1,2,128,128]{3,2,1,0:T(8,128)}, f32[1,2,128,128]{3,2,1,0:T(8,128)S(1)}, u32[]{:S(2)}) copy-start(f32[1,2,128,128]{3,2,1,0:T(8,128)S(1)} %multiply_add_fusion) | copy-start | bytes 393220
  186.5 34.1 %copy-start.17 = (f32[32]{0:T(128)S(1)}, f32[32]{0:T(128)}, u32[]{:S(2)}) copy-start(f32[32]{0:T(128)} %param.40) | copy-start | bytes 388
  209.3 29.1 %copy-start.6 = (bf16[32,640]{1,0:T(8,128)(2,1)S(1)}, bf16[32,640]{1,0:T(8,128)(2,1)}, u32[]{:S(2)}) copy-start(bf16[32,640]{1,0:T(8,128)(2,1)} %param.42) | copy-start | bytes 122884
  221.3 8.5 %all-to-all-start.11 = ((bf16[8,1,32]{2,1,0:T(2,128)(2,1)}), bf16[8,1,32]{2,1,0:T(2,128)(2,1)S(1)}, u32[]{:S(2)}, u32[]{:S(2)}) async-start(bf16[8,1,32]{2,1,0:T(2,128)(2,1)} %broadcast_in_dim.25), calls=%async_computation.11 | async-start | bytes 8192 | tf_op jit(solution)/shard_map/all_to_all | solution.py:16
  225.3 13.5 %copy-start.7 = (bf16[32,640]{1,0:T(8,128)(2,1)S(1)}, bf16[32,640]{1,0:T(8,128)(2,1)}, u32[]{:S(2)}) copy-start(bf16[32,640]{1,0:T(8,128)(2,1)} %param.41) | copy-start | bytes 122884
  229.8 8.6 %all-to-all-start.10 = ((bf16[8,2,512]{2,1,0:T(2,128)(2,1)}), bf16[8,2,512]{2,1,0:T(2,128)(2,1)S(1)}, u32[]{:S(2)}, u32[]{:S(2)}) async-start(bf16[8,2,512]{2,1,0:T(2,128)(2,1)} %reshape.582), calls=%async_computation.10 | async-start | bytes 32768 | tf_op jit(solution)/shard_map/all_to_all | solution.py:16
  282.4 29.7 %copy-start.4 = (bf16[640,32]{0,1:T(8,128)(2,1)S(1)}, bf16[640,32]{0,1:T(8,128)(2,1)}, u32[]{:S(2)}) copy-start(bf16[640,32]{0,1:T(8,128)(2,1)} %param.43) | copy-start | bytes 122884
where the time goes:
time: 326 us; the launch traced here: 325 us
  blocking collectives  210 us (64%)
  waiting for transfers between devices  57 us (17%)
  starting transfers between devices  34.5 us (11%)
  local copies, waits for them, and re-layouts  12.3 us (4%)
  other arithmetic  4.78 us (1%)
  matrix products  4.46 us (1%)
    all_to_all x5, blocking collectives, sent_and_summed(): pieces = lax.all_to_all(cut_along(x, dim, count), axis, 0, 0, tiled=True)  128 us
    all_to_all x3, blocking collectives, from_everyone(): lax.all_to_all(jnp.broadcast_to(x[None], (count, *x.shape)), axis, 0, 0,...  81.6 us
    all_to_all x1, waiting for transfers between devices, sent_and_summed(): pieces = lax.all_to_all(cut_along(x, dim, count), axis, 0, 0, tiled=True)  32.5 us
    all_to_all x6, starting transfers between devices, from_everyone(): lax.all_to_all(jnp.broadcast_to(x[None], (count, *x.shape)), axis, 0, 0,...  29.7 us
    all_to_all x6, waiting for transfers between devices, from_everyone(): lax.all_to_all(jnp.broadcast_to(x[None], (count, *x.shape)), axis, 0, 0,...  24.6 us
  transfers between devices with their start and end apart: 7, of which 7 were waited for; matrix products, arithmetic and copies ran while one was open for 1% of the time, Pallas kernels for 0%

commit v1 on v0

v1 whole, which is shorter than its diff:
```python
import jax
import jax.numpy as jnp
from jax import lax
from jax.sharding import Mesh, PartitionSpec as P

D = 2048
HEAD_DIM = 128
NEW = 4
EPS = 1e-06

NZ, NY, NX, NC = 16, 4, 4, 2
F32 = jnp.float32
BF16 = jnp.bfloat16


def exchange(x, axes):
    return lax.all_to_all(x, axes, 0, 0, tiled=True)


def to_all(x, axes):
    count = lax.axis_size(axes)
    return exchange(jnp.broadcast_to(x[None], (count, *x.shape)), axes)


def dot(a, b):
    return jnp.dot(a, b, preferred_element_type=F32)


def exchange_weights(parts):
    flat = jnp.concatenate([p.reshape(NY, -1) for p in parts], axis=1)
    flat = jnp.pad(flat, ((0, 0), (0, -flat.shape[1] % 1024)))
    width = flat.shape[1]
    both = jnp.broadcast_to(flat[:, None], (NY, NC, width)).reshape(NY * NC, width // 128, 128)
    got = exchange(both, ("y", "c")).reshape(NY, NC, width)
    out, at = [], 0
    for p in parts:
        size = p.shape[1] * p.shape[2]
        out.append(got[:, :, at : at + size].reshape(NY, NC, p.shape[1], p.shape[2]))
        at += size
    return out


def in_three(x):
    first = lax.reduce_precision(x, 8, 7)
    second = lax.reduce_precision(x - first, 8, 7)
    third = x - first - second
    return jnp.concatenate([first, second, third]).astype(BF16)


def up_parts(w):
    return w.reshape(32, NY, 160).transpose(1, 0, 2)


def up_weight(gate, up):
    gate = gate.transpose(0, 2, 1, 3).reshape(128, 320)
    up = up.transpose(0, 2, 1, 3).reshape(128, 320)
    gap = jnp.zeros((128, 64), BF16)
    return jnp.concatenate([gate, gap, up, gap], axis=1)


def down_weight(down):
    down = down.transpose(1, 2, 0, 3).reshape(320, 128)
    return jnp.concatenate([down, jnp.zeros((64, 128), BF16)], axis=0)


def projected(resid, gain, weight, spot):
    wide = resid.astype(F32)
    squares = jnp.sum(wide * wide, axis=1, keepdims=True)
    out = dot((wide * gain[None]).astype(BF16), weight)
    column = lax.broadcasted_iota(jnp.int32, out.shape, 1)
    out = jnp.where(column == spot, squares, out).astype(BF16)
    got = exchange(out.reshape(NZ, 8, -1), "z")
    total = jnp.sum(got.astype(F32), axis=0)
    scale = lax.rsqrt(total[:, spot : spot + 1] / D + EPS)
    return total, scale


def half(resid, gain, w_up, w_down):
    total, scale = projected(resid, gain, w_up, 320)
    hidden = (jax.nn.silu(total[:, :384] * scale) * (total[:, 384:] * scale)).astype(BF16)
    hidden = to_all(hidden, "z").reshape(128, 384)
    return dot(hidden, w_down)


def advance(q, k, v, z, beta_logit, decay_logit, state_now, length, decay_rate, decay_bias, head_gain):
    query = jax.nn.silu(q)
    query = (
        query * lax.rsqrt(jnp.sum(query * query, axis=-1, keepdims=True) + EPS) * HEAD_DIM ** (-0.5)
    )
    keyvec = jax.nn.silu(k)
    keyvec = keyvec * lax.rsqrt(jnp.sum(keyvec * keyvec, axis=-1, keepdims=True) + EPS)
    values = jax.nn.silu(v)
    live = (jnp.arange(NEW, dtype=jnp.int32) < length).astype(F32)[:, None]
    beta = jax.nn.sigmoid(beta_logit) * live
    decay = jnp.exp(-decay_rate * jax.nn.softplus(decay_logit + decay_bias) * live)
    outputs = []
    for t in range(NEW):
        state_now = state_now * decay[t][:, None, None]
        predicted = jnp.sum(keyvec[t][:, :, None] * state_now, axis=1)
        update = beta[t][:, None] * (values[t] - predicted)
        state_now = state_now + keyvec[t][:, :, None] * update[:, None, :]
        outputs.append(jnp.sum(query[t][:, :, None] * state_now, axis=1))
    mixed = jnp.stack(outputs, axis=0) * live[..., None]
    mixed = mixed * lax.rsqrt(jnp.mean(mixed * mixed, axis=-1, keepdims=True) + EPS) * head_gain
    mixed = mixed * jax.nn.silu(z)
    return mixed.reshape(NEW, -1).astype(BF16), state_now


def on_device(
    tokens,
    lengths,
    memory_state,
    gain_first,
    first_gate,
    first_up,
    first_down,
    gain_mixer,
    query_weight,
    key_weight,
    value_weight,
    outgate_weight,
    beta_weight,
    decay_weight,
    decay_rate,
    decay_bias,
    head_gain,
    out_weight,
    gain_second,
    second_gate,
    second_up,
    second_down,
):
    tp = lax.axis_index(("x", "c"))
    logits = jnp.concatenate(
        [
            lax.dynamic_slice_in_dim(beta_weight, tp * 2, 2, 1),
            lax.dynamic_slice_in_dim(decay_weight, tp * 2, 2, 1),
        ],
        axis=1,
    )
    gains = jnp.stack([gain_first, gain_mixer, gain_second])
    parts = [
        up_parts(first_gate),
        up_parts(first_up),
        first_down.reshape(NY, 160, 32),
        jnp.stack([query_weight, key_weight, value_weight, outgate_weight]),
        up_parts(second_gate),
        up_parts(second_up),
        second_down.reshape(NY, 160, 32),
        jnp.broadcast_to(logits[None], (NY, 32, 4)),
        jnp.broadcast_to(in_three(gains)[None], (NY, 9, 32)),
    ]
    gate1, up1, down1, mix, gate2, up2, down2, logit, gains = exchange_weights(parts)
    w_up1, w_down1 = up_weight(gate1, up1), down_weight(down1)
    w_up2, w_down2 = up_weight(gate2, up2), down_weight(down2)
    w_mix = jnp.concatenate(
        [
            mix.transpose(0, 2, 1, 3).reshape(128, 512),
            logit.transpose(0, 2, 1, 3).reshape(128, 8),
            jnp.zeros((128, 120), BF16),
        ],
        axis=1,
    )
    gains = jnp.sum(gains[:, 0].astype(F32).reshape(NY, 3, 3, 32), axis=1)
    gains = gains.transpose(1, 0, 2).reshape(3, 128)

    sent = tokens.reshape(2, NC, 8 * 32).transpose(1, 0, 2).reshape(NC, 512)
    sent = jnp.broadcast_to(sent[None], (NY * NX, NC, 512)).reshape(32, 4, 128)
    got = exchange(sent, ("y", "x", "c")).reshape(NY, NX * NC * 16, 32)
    resid = got.transpose(1, 0, 2).reshape(128, 128)

    branch = half(resid, gains[0], w_up1, w_down1)
    pieces = to_all(branch.astype(BF16), ("y", "x"))
    branch = jnp.sum(pieces.astype(F32), axis=0)
    resid = (resid.astype(F32) + 0.5 * branch).astype(BF16)

    total, scale = projected(resid, gains[1], w_mix, 520)
    total = total * scale
    wide = total[:, :512].reshape(2, NEW, NC, 256).transpose(0, 2, 1, 3)
    small = total[:, 512:520].reshape(2, NEW, NC, 4).transpose(0, 2, 1, 3)
    small = jnp.pad(small, ((0, 0), (0, 0), (0, 0), (0, 124)))
    sent = jnp.concatenate([wide, small], axis=3)
    sent = jnp.broadcast_to(sent[None], (2, 2, NC, NEW, 384)).reshape(NY * NC, 12, 128)
    got = exchange(sent, ("y", "c")).reshape(NY, NC, NEW, 384)
    got = lax.dynamic_index_in_dim(got, lax.axis_index("y") // 2, 1, keepdims=False)
    heads = got[:, :, :256].reshape(4, NEW, 2, HEAD_DIM)
    small = got[0, :, 256:260]
    mixed, state_out = advance(
        heads[0],
        heads[1],
        heads[2],
        heads[3],
        small[:, 0:2],
        small[:, 2:4],
        memory_state[0],
        lengths[0],
        decay_rate,
        decay_bias,
        head_gain,
    )
    everyone = to_all(mixed, ("z", "y"))
    everyone = everyone.reshape(NZ, NC, 8, 256).transpose(1, 0, 2, 3).reshape(NC * 128, 256)
    part = lax.dot_general(
        out_weight, everyone, (((0,), (1,)), ((), ())), preferred_element_type=F32
    ).astype(BF16)
    part = part.reshape(32, NC, 128).transpose(1, 0, 2)
    sent = jnp.broadcast_to(part[None], (NY * NX, NC, 32, 128)).reshape(32, 32, 128)
    got = exchange(sent, ("y", "x", "c")).reshape(NY, NX * NC, 32, 128)
    branch = jnp.sum(got.astype(F32), axis=1).reshape(128, 128).T
    resid = (resid.astype(F32) + branch).astype(BF16)

    branch = half(resid, gains[2], w_up2, w_down2)
    both = jnp.stack([branch.astype(BF16), resid])
    both = both.reshape(2, NX * NC, 16, NY, 32).transpose(3, 1, 0, 2, 4).reshape(32, 8, 128)
    got = exchange(both, ("y", "x", "c")).reshape(NY * NX, NC, 2, 16, 32)
    branch = jnp.sum(got[:, :, 0].astype(F32), axis=0)
    out = (got[0, :, 1].astype(F32) + 0.5 * branch).astype(BF16)
    out = out.reshape(NC, 2, 8, 32).transpose(1, 0, 2, 3).reshape(32, 32)
    return out, state_out[None]


def solution(mesh):
    fine = Mesh(mesh.devices.reshape(NZ, NY, NX, NC), ("z", "y", "x", "c"))
    kv, tp = ("z", "y"), ("x", "c")
    in_specs = (
        P(tp, kv),
        P(kv),
        P(kv, tp, None, None),
        P(kv),
        P(kv, tp),
        P(kv, tp),
        P(tp, kv),
        P(kv),
        P(kv, tp),
        P(kv, tp),
        P(kv, tp),
        P(kv, tp),
        P(kv, None),
        P(kv, None),
        P(tp),
        P(tp),
        P(),
        P(tp, kv),
        P(kv),
        P(kv, tp),
        P(kv, tp),
        P(tp, kv),
    )
    out_specs = (P(tp, kv), P(kv, tp, None, None))
    return jax.shard_map(
        on_device, mesh=fine, in_specs=in_specs, out_specs=out_specs, check_vma=False
    )
```

time: 326 us -> 232 us (0.71)
  blocking collectives: 210 us -> 60.9 us
  starting transfers between devices: 34.5 us -> 65 us
  local copies, waits for them, and re-layouts: 12.3 us -> 25.7 us
  waiting for transfers between devices: 57 us -> 70.2 us
    all_to_all x8 -> x3, blocking collectives: 210 us -> 60.9 us  [exchange(): return lax.all_to_all(x, axes, 0, 0, tiled=True)]
    all_to_all x7 -> x9, starting transfers between devices: 34.5 us -> 65 us  [exchange(): return lax.all_to_all(x, axes, 0, 0, tiled=True)]
    all_to_all x7 -> x9, waiting for transfers between devices: 57 us -> 70.2 us  [exchange(): return lax.all_to_all(x, axes, 0, 0, tiled=True)]
    reshape x12 -> x43, local copies, waits for them, and re-layouts: 0.76 us -> 8.46 us  [the longest x12 1.85 us: exchange_weights(): out.append(got[:, :, at:at + size].reshape(NY, NC, p.shape[1], p.shape[2]))]
    concatenate x12 -> x4, local copies, waits for them, and re-layouts: 3.46 us -> 0.2 us  [the longest x1 0.1 us: on_device(): jnp.concatenate([lax.dynamic_slice_in_dim(beta_weight, tp * 2, 2, 1), lax...]
    unnamed x55 -> x52, local copies, waits for them, and re-layouts: 4.81 us -> 8.02 us
  transfers between devices with their start and end apart: 7 -> 9, of which waited for: 7 -> 8; matrix products, arithmetic and copies ran while one was open for 1% -> 4% of each run, Pallas kernels for 0% -> 0%
where the time goes in v1:
time: 232 us; the launch traced here: 230 us
  waiting for transfers between devices  70.2 us (30%)
  starting transfers between devices  65 us (28%)
  blocking collectives  60.9 us (26%)
  local copies, waits for them, and re-layouts  25.7 us (11%)
  other arithmetic  4.53 us (2%)
    all_to_all x9, waiting for transfers between devices, exchange(): return lax.all_to_all(x, axes, 0, 0, tiled=True)  70.2 us
    all_to_all x9, starting transfers between devices, exchange(): return lax.all_to_all(x, axes, 0, 0, tiled=True)  65 us
    all_to_all x3, blocking collectives, exchange(): return lax.all_to_all(x, axes, 0, 0, tiled=True)  60.9 us
    unnamed x52, local copies, waits for them, and re-layouts  8.02 us
  transfers between devices with their start and end apart: 9, of which 8 were waited for; matrix products, arithmetic and copies ran while one was open for 4% of the time, Pallas kernels for 0%

profile of v1, /device:TPU:1, one launch (start us, length us, event | category | flops | bytes accessed | tf_op | source)
XLA Modules:
  0.0 230.5 jit_solution(17035599761573511409)
XLA Ops:
  0.6 0.8 reshape.599
  1.5 0.6 reshape.600
  2.1 10.5 %all-to-all-start = ((bf16[32,4,128]{2,1,0:T(4,128)(2,1)}), bf16[32,4,128]{2,1,0:T(4,128)(2,1)S(1)}, u32[]{:S(2)}, u32[]{:S(2)}) async-start(bf16[32,4,128]{2,1,0:T(4,128)(2,1)} %reshape.600), calls=%async_computation | async-start | bytes 65536 | tf_op jit(solution)/shard_map/all_to_all | solution.py:17
  12.9 0.7 copy-done.4
  13.9 0.6 copy-done.7
  14.7 0.2 reshape_reshape.6
  14.9 0.5 copy-done.9
  15.5 0.7 copy-done.10
  16.2 0.7 copy-done.11
  17.0 0.7 copy-done.5
  17.9 0.6 copy-done.6
  18.9 0.6 copy-done.8
  19.6 0.2 reshape_reshape.7
  19.9 0.7 constant_dynamic-slice_fusion
  20.8 0.6 copy-done.13
  22.1 0.3 broadcast_in_dim.55
  22.4 1.2 reshape.609
  23.7 4.9 %all-to-all-start.1 = ((bf16[8,312,128]{2,1,0:T(8,128)(2,1)}), bf16[8,312,128]{2,1,0:T(8,128)(2,1)S(1)}, u32[]{:S(2)}, u32[]{:S(2)}) async-start(bf16[8,312,128]{2,1,0:T(8,128)(2,1)} %reshape.609), calls=%async_computation.1 | async-start | bytes 1277952 | tf_op jit(solution)/shard_map/all_to_all | solution.py:17
  28.8 10.3 %all-to-all-done.1 = bf16[8,312,128]{2,1,0:T(8,128)(2,1)S(1)} async-done(((bf16[8,312,128]{2,1,0:T(8,128)(2,1)}), bf16[8,312,128]{2,1,0:T(8,128)(2,1)S(1)}, u32[]{:S(2)}, u32[]{:S(2)}) %all-to-all-start.1) | async-done | bytes 639008 | tf_op jit(solution)/shard_map/all_to_all | solution.py:17
  39.3 0.3 fusion.74
  39.7 0.5 copy-done.1
  41.0 0.6 slice-done
  41.8 0.3 fusion.4
  42.1 25.2 %all_to_all.60 = bf16[16,8,768]{2,1,0:T(8,128)(2,1)S(1)} all-to-all(bf16[16,8,768]{2,1,0:T(8,128)(2,1)S(1)} %fusion.4), channel_id=1, replica_groups=mesh['z'=16,'y'=4,'x'=4,'c'=2] {'z'}, dimensions={0} | all-to-all | bytes 393216 | tf_op jit(solution)/shard_map/all_to_all | solution.py:17
  67.6 0.7 broadcast_in_dim.56
  68.3 9.1 %all-to-all-start.3 = ((bf16[16,8,384]{2,1,0:T(8,128)(2,1)}), bf16[16,8,384]{2,1,0:T(8,128)(2,1)S(1)}, u32[]{:S(2)}, u32[]{:S(2)}) async-start(bf16[16,8,384]{2,1,0:T(8,128)(2,1)} %broadcast_in_dim.56), calls=%async_computation.3 | async-start | bytes 196608 | tf_op jit(solution)/shard_map/all_to_all | solution.py:17
  77.3 0.2 reshape.618
  77.5 0.2 copy.182
  77.9 11.3 %all-to-all-done.3 = bf16[16,8,384]{2,1,0:T(8,128)(2,1)S(1)} async-done(((bf16[16,8,384]{2,1,0:T(8,128)(2,1)}), bf16[16,8,384]{2,1,0:T(8,128)(2,1)S(1)}, u32[]{:S(2)}, u32[]{:S(2)}) %all-to-all-start.3) | async-done | bytes 98336 | tf_op jit(solution)/shard_map/all_to_all | solution.py:17
  89.4 0.9 broadcast_in_dim.57
  90.3 4.7 %all-to-all-start.4 = ((bf16[16,128,128]{2,1,0:T(8,128)(2,1)}), bf16[16,128,128]{2,1,0:T(8,128)(2,1)S(1)}, u32[]{:S(2)}, u32[]{:S(2)}) async-start(bf16[16,128,128]{2,1,0:T(8,128)(2,1)} %broadcast_in_dim.57), calls=%async_computation.4 | async-start | bytes 1048576 | tf_op jit(solution)/shard_map/all_to_all | solution.py:17
  95.2 0.7 slice-done.1
  96.3 0.4 slice-done.2
  96.8 7.1 %all-to-all-done.4 = bf16[16,128,128]{2,1,0:T(8,128)(2,1)S(1)} async-done(((bf16[16,128,128]{2,1,0:T(8,128)(2,1)}), bf16[16,128,128]{2,1,0:T(8,128)(2,1)S(1)}, u32[]{:S(2)}, u32[]{:S(2)}) %all-to-all-start.4) | async-done | bytes 524320 | tf_op jit(solution)/shard_map/all_to_all | solution.py:17
  104.2 0.9 fusion.5
  105.0 6.1 %all-to-all-start.5 = ((bf16[16,8,640]{2,1,0:T(8,128)(2,1)}), bf16[16,8,640]{2,1,0:T(8,128)(2,1)S(1)}, u32[]{:S(2)}, u32[]{:S(2)}) async-start(bf16[16,8,640]{2,1,0:T(8,128)(2,1)} %fusion.5), calls=%async_computation.5 | async-start | bytes 327680 | tf_op jit(solution)/shard_map/all_to_all | solution.py:17
  111.9 11.5 %all-to-all-done.5 = bf16[16,8,640]{2,1,0:T(8,128)(2,1)S(1)} async-done(((bf16[16,8,640]{2,1,0:T(8,128)(2,1)}), bf16[16,8,640]{2,1,0:T(8,128)(2,1)S(1)}, u32[]{:S(2)}, u32[]{:S(2)}) %all-to-all-start.5) | async-done | bytes 163872 | tf_op jit(solution)/shard_map/all_to_all | solution.py:17
  123.4 0.2 fusion.46
  123.8 0.6 reshape.627
  124.5 8.2 %all-to-all-start.6 = ((f32[8,12,128]{2,1,0:T(8,128)}), f32[8,12,128]{2,1,0:T(8,128)S(1)}, u32[]{:S(2)}, u32[]{:S(2)}) async-start(f32[8,12,128]{2,1,0:T(8,128)} %reshape.627), calls=%async_computation.6 | async-start | bytes 131072 | tf_op jit(solution)/shard_map/all_to_all | solution.py:17
  132.7 0.7 copy-done.18
  133.4 4.2 %all-to-all-done.6 = f32[8,12,128]{2,1,0:T(8,128)S(1)} async-done(((f32[8,12,128]{2,1,0:T(8,128)}), f32[8,12,128]{2,1,0:T(8,128)S(1)}, u32[]{:S(2)}, u32[]{:S(2)}) %all-to-all-start.6) | async-done | bytes 49184 | tf_op jit(solution)/shard_map/all_to_all | solution.py:17
  137.8 0.4 copy-done.16
  138.8 0.2 multiply_reduce_fusion.6
  139.0 0.2 multiply_reduce_fusion.3
  139.3 0.2 multiply_reduce_fusion.2
  139.6 0.2 multiply_reduce_fusion.4
  140.2 19.9 %all_to_all.61 = bf16[64,4,256]{2,1,0:T(4,128)(2,1)S(1)} all-to-all(bf16[64,4,256]{2,1,0:T(4,128)(2,1)S(1)} %broadcast_in_dim.62), channel_id=1, replica_groups=mesh['z'=16,'y'=4,'x'=4,'c'=2] {'z','y'}, dimensions={0} | all-to-all | bytes 262144 | tf_op jit(solution)/shard_map/all_to_all | solution.py:17
  160.4 0.7 broadcast_in_dim.63
  161.2 7.0 %all-to-all-start.8 = ((bf16[32,32,128]{2,1,0:T(8,128)(2,1)}), bf16[32,32,128]{2,1,0:T(8,128)(2,1)S(1)}, u32[]{:S(2)}, u32[]{:S(2)}) async-start(bf16[32,32,128]{2,1,0:T(8,128)(2,1)} %bitcast.64), calls=%async_computation.8 | async-start | bytes 524288 | tf_op jit(solution)/shard_map/all_to_all | solution.py:17
  169.1 8.0 %all-to-all-done.8 = bf16[32,32,128]{2,1,0:T(8,128)(2,1)S(1)} async-done(((bf16[32,32,128]{2,1,0:T(8,128)(2,1)}), bf16[32,32,128]{2,1,0:T(8,128)(2,1)S(1)}, u32[]{:S(2)}, u32[]{:S(2)}) %all-to-all-start.8) | async-done | bytes 262176 | tf_op jit(solution)/shard_map/all_to_all | solution.py:17
  177.4 0.3 fusion.3
  177.7 15.8 %all_to_all.62 = bf16[16,8,768]{2,1,0:T(8,128)(2,1)S(1)} all-to-all(bf16[16,8,768]{2,1,0:T(8,128)(2,1)S(1)} %fusion.3), channel_id=1, replica_groups=mesh['z'=16,'y'=4,'x'=4,'c'=2] {'z'}, dimensions={0} | all-to-all | bytes 393216 | tf_op jit(solution)/shard_map/all_to_all | solution.py:17
  193.8 0.7 broadcast_in_dim.65
  194.5 8.3 %all-to-all-start.10 = ((bf16[16,8,384]{2,1,0:T(8,128)(2,1)}), bf16[16,8,384]{2,1,0:T(8,128)(2,1)S(1)}, u32[]{:S(2)}, u32[]{:S(2)}) async-start(bf16[16,8,384]{2,1,0:T(8,128)(2,1)} %broadcast_in_dim.65), calls=%async_computation.10 | async-start | bytes 196608 | tf_op jit(solution)/shard_map/all_to_all | solution.py:17
  202.7 0.2 reshape.640
  202.9 0.2 copy.194
  203.4 11.2 %all-to-all-done.10 = bf16[16,8,384]{2,1,0:T(8,128)(2,1)S(1)} async-done(((bf16[16,8,384]{2,1,0:T(8,128)(2,1)}), bf16[16,8,384]{2,1,0:T(8,128)(2,1)S(1)}, u32[]{:S(2)}, u32[]{:S(2)}) %all-to-all-start.10) | async-done | bytes 98336 | tf_op jit(solution)/shard_map/all_to_all | solution.py:17
  214.9 0.2 maximum_bitcast_fusion
  215.2 0.8 reshape.642
  216.0 6.2 %all-to-all-start.11 = ((bf16[32,8,128]{2,1,0:T(8,128)(2,1)}), bf16[32,8,128]{2,1,0:T(8,128)(2,1)S(1)}, u32[]{:S(2)}, u32[]{:S(2)}) async-start(bf16[32,8,128]{2,1,0:T(8,128)(2,1)} %reshape.642), calls=%async_computation.11 | async-start | bytes 131072 | tf_op jit(solution)/shard_map/all_to_all | solution.py:17
  222.2 0.9 multiply_add_fusion
  223.1 6.6 %all-to-all-done.11 = bf16[32,8,128]{2,1,0:T(8,128)(2,1)S(1)} async-done(((bf16[32,8,128]{2,1,0:T(8,128)(2,1)}), bf16[32,8,128]{2,1,0:T(8,128)(2,1)S(1)}, u32[]{:S(2)}, u32[]{:S(2)}) %all-to-all-start.11) | async-done | bytes 65568 | tf_op jit(solution)/shard_map/all_to_all | solution.py:17
  229.9 0.6 copy.197
  (170 shorter events, 9.5 us)
Async XLA Ops:
  0.6 159.6 %copy-start = (bf16[256,32]{0,1:T(8,128)(2,1)S(1)}, bf16[256,32]{0,1:T(8,128)(2,1)}, u32[]{:S(2)}) copy-start(bf16[256,32]{0,1:T(8,128)(2,1)} %param.39) | copy-start | bytes 49156
  2.1 10.5 %copy-start.3 = (bf16[32,640]{1,0:T(8,128)(2,1)S(1)}, bf16[32,640]{1,0:T(8,128)(2,1)}, u32[]{:S(2)}) copy-start(bf16[32,640]{1,0:T(8,128)(2,1)} %param.26) | copy-start | bytes 122884
  2.1 21.6 %all-to-all-start = ((bf16[32,4,128]{2,1,0:T(4,128)(2,1)}), bf16[32,4,128]{2,1,0:T(4,128)(2,1)S(1)}, u32[]{:S(2)}, u32[]{:S(2)}) async-start(bf16[32,4,128]{2,1,0:T(4,128)(2,1)} %reshape.600), calls=%async_computation | async-start | bytes 65536 | tf_op jit(solution)/shard_map/all_to_all | solution.py:17
  12.9 0.8 copy-start.4
  13.8 0.8 copy-start.7
  14.7 0.7 copy-start.9
  15.4 0.7 copy-start.10
  16.2 0.7 copy-start.11
  16.2 0.7 copy-start.12
  16.9 0.8 copy-start.5
  17.8 0.8 copy-start.6
  18.7 0.8 copy-start.8
  20.8 0.7 copy-start.13
  20.8 0.7 copy-start.14
  20.8 0.7 copy-start.15
  23.7 15.5 %all-to-all-start.1 = ((bf16[8,312,128]{2,1,0:T(8,128)(2,1)}), bf16[8,312,128]{2,1,0:T(8,128)(2,1)S(1)}, u32[]{:S(2)}, u32[]{:S(2)}) async-start(bf16[8,312,128]{2,1,0:T(8,128)(2,1)} %reshape.609), calls=%async_computation.1 | async-start | bytes 1277952 | tf_op jit(solution)/shard_map/all_to_all | solution.py:17
  39.3 0.8 copy-start.1
  40.9 0.7 slice-start
  68.3 20.9 %all-to-all-start.3 = ((bf16[16,8,384]{2,1,0:T(8,128)(2,1)}), bf16[16,8,384]{2,1,0:T(8,128)(2,1)S(1)}, u32[]{:S(2)}, u32[]{:S(2)}) async-start(bf16[16,8,384]{2,1,0:T(8,128)(2,1)} %broadcast_in_dim.56), calls=%async_computation.3 | async-start | bytes 196608 | tf_op jit(solution)/shard_map/all_to_all | solution.py:17
  90.3 13.7 %all-to-all-start.4 = ((bf16[16,128,128]{2,1,0:T(8,128)(2,1)}), bf16[16,128,128]{2,1,0:T(8,128)(2,1)S(1)}, u32[]{:S(2)}, u32[]{:S(2)}) async-start(bf16[16,128,128]{2,1,0:T(8,128)(2,1)} %broadcast_in_dim.57), calls=%async_computation.4 | async-start | bytes 1048576 | tf_op jit(solution)/shard_map/all_to_all | solution.py:17
  95.2 0.7 slice-start.1
  95.8 0.9 slice-start.2
  105.0 18.3 %all-to-all-start.5 = ((bf16[16,8,640]{2,1,0:T(8,128)(2,1)}), bf16[16,8,640]{2,1,0:T(8,128)(2,1)S(1)}, u32[]{:S(2)}, u32[]{:S(2)}) async-start(bf16[16,8,640]{2,1,0:T(8,128)(2,1)} %fusion.5), calls=%async_computation.5 | async-start | bytes 327680 | tf_op jit(solution)/shard_map/all_to_all | solution.py:17
  111.2 0.7 copy-start.17
  124.5 13.1 %all-to-all-start.6 = ((f32[8,12,128]{2,1,0:T(8,128)}), f32[8,12,128]{2,1,0:T(8,128)S(1)}, u32[]{:S(2)}, u32[]{:S(2)}) async-start(f32[8,12,128]{2,1,0:T(8,128)} %reshape.627), calls=%async_computation.6 | async-start | bytes 131072 | tf_op jit(solution)/shard_map/all_to_all | solution.py:17
  132.7 0.7 copy-start.18
  137.6 0.7 copy-start.16
  137.6 1.0 copy-start.2
  161.2 16.0 %all-to-all-start.8 = ((bf16[32,32,128]{2,1,0:T(8,128)(2,1)}), bf16[32,32,128]{2,1,0:T(8,128)(2,1)S(1)}, u32[]{:S(2)}, u32[]{:S(2)}) async-start(bf16[32,32,128]{2,1,0:T(8,128)(2,1)} %bitcast.64), calls=%async_computation.8 | async-start | bytes 524288 | tf_op jit(solution)/shard_map/all_to_all | solution.py:17
  194.5 20.1 %all-to-all-start.10 = ((bf16[16,8,384]{2,1,0:T(8,128)(2,1)}), bf16[16,8,384]{2,1,0:T(8,128)(2,1)S(1)}, u32[]{:S(2)}, u32[]{:S(2)}) async-start(bf16[16,8,384]{2,1,0:T(8,128)(2,1)} %broadcast_in_dim.65), calls=%async_computation.10 | async-start | bytes 196608 | tf_op jit(solution)/shard_map/all_to_all | solution.py:17
  216.0 13.7 %all-to-all-start.11 = ((bf16[32,8,128]{2,1,0:T(8,128)(2,1)}), bf16[32,8,128]{2,1,0:T(8,128)(2,1)S(1)}, u32[]{:S(2)}, u32[]{:S(2)}) async-start(bf16[32,8,128]{2,1,0:T(8,128)(2,1)} %reshape.642), calls=%async_computation.11 | async-start | bytes 131072 | tf_op jit(solution)/shard_map/all_to_all | solution.py:17

commit v2 on v1

v2 whole, which is shorter than its diff:
```python
import jax
import jax.numpy as jnp
from jax import lax
from jax.sharding import Mesh, PartitionSpec as P

D = 2048
HEAD_DIM = 128
NEW = 4
EPS = 1e-06

NZ, NY, NX, NC = 16, 4, 4, 2
F32 = jnp.float32
BF16 = jnp.bfloat16


def exchange(x, axes):
    return lax.all_to_all(x, axes, 0, 0, tiled=True)


def to_all(x, axes):
    count = lax.axis_size(axes)
    return exchange(jnp.broadcast_to(x[None], (count, *x.shape)), axes)


def dot(a, b):
    return jnp.dot(a, b, preferred_element_type=F32)


def in_three(x):
    first = lax.reduce_precision(x, 8, 7)
    second = lax.reduce_precision(x - first, 8, 7)
    third = x - first - second
    return jnp.concatenate([first, second, third], axis=1).astype(BF16)


def gather_weights(pieces):
    own = jnp.concatenate(pieces, axis=1)
    own = jnp.pad(own, ((0, 0), (0, -own.shape[1] % 128)))
    return to_all(own, "y").reshape(128, -1)


def projected(resid, gain, weight, tail):
    wide = resid.astype(F32)
    squares = jnp.sum(wide * wide, axis=1, keepdims=True)
    operand = (wide * gain).astype(BF16)
    out = dot(operand, weight).astype(BF16)
    column = lax.broadcasted_iota(jnp.int32, (64, 128), 1)
    if tail is None:
        last = jnp.where(column == 127, squares, 0.0)
    else:
        last = jnp.where(column == 127, squares, dot(operand, tail))
    out = jnp.concatenate([out, last.astype(BF16)], axis=1)
    got = exchange(out.reshape(NZ, NEW, -1), "z")
    total = jnp.sum(got.astype(F32), axis=0)
    scale = lax.rsqrt(total[:, -1:] / D + EPS)
    return total[:, :-128] * scale, total[:, -128:] * scale


def half(resid, gain, w_up, w_down):
    total, _ = projected(resid, gain, w_up, None)
    hidden = (jax.nn.silu(total[:, :640]) * total[:, 640:]).astype(BF16)
    hidden = to_all(hidden, "z").reshape(64, 640)
    return lax.dot_general(hidden, w_down, (((1,), (1,)), ((), ())), preferred_element_type=F32)


def advance(q, k, v, z, beta_logit, decay_logit, state_now, length, decay_rate, decay_bias, head_gain):
    query = jax.nn.silu(q)
    query = (
        query * lax.rsqrt(jnp.sum(query * query, axis=-1, keepdims=True) + EPS) * HEAD_DIM ** (-0.5)
    )
    keyvec = jax.nn.silu(k)
    keyvec = keyvec * lax.rsqrt(jnp.sum(keyvec * keyvec, axis=-1, keepdims=True) + EPS)
    values = jax.nn.silu(v)
    live = (jnp.arange(NEW, dtype=jnp.int32) < length).astype(F32)[:, None]
    beta = jax.nn.sigmoid(beta_logit) * live
    decay = jnp.exp(-decay_rate * jax.nn.softplus(decay_logit + decay_bias) * live)
    outputs = []
    for t in range(NEW):
        state_now = state_now * decay[t][:, None, None]
        predicted = jnp.sum(keyvec[t][:, :, None] * state_now, axis=1)
        update = beta[t][:, None] * (values[t] - predicted)
        state_now = state_now + keyvec[t][:, :, None] * update[:, None, :]
        outputs.append(jnp.sum(query[t][:, :, None] * state_now, axis=1))
    mixed = jnp.stack(outputs, axis=0) * live[..., None]
    mixed = mixed * lax.rsqrt(jnp.mean(mixed * mixed, axis=-1, keepdims=True) + EPS) * head_gain
    mixed = mixed * jax.nn.silu(z)
    return mixed.reshape(NEW, -1).astype(BF16), state_now


def on_device(
    tokens,
    lengths,
    memory_state,
    gain_first,
    first_gate,
    first_up,
    first_down,
    gain_mixer,
    query_weight,
    key_weight,
    value_weight,
    outgate_weight,
    beta_weight,
    decay_weight,
    decay_rate,
    decay_bias,
    head_gain,
    out_weight,
    gain_second,
    second_gate,
    second_up,
    second_down,
):
    gains = jnp.stack([gain_first, gain_mixer, gain_second], axis=1)
    first = gather_weights([first_gate, first_up, first_down.T, in_three(gains)])
    rest = gather_weights(
        [
            query_weight,
            key_weight,
            value_weight,
            outgate_weight,
            out_weight.T,
            second_gate,
            second_up,
            second_down.T,
            beta_weight,
            decay_weight,
        ]
    )
    gains = jnp.sum(first[:, 1920:1929].astype(F32).T.reshape(3, 3, 128), axis=0)

    sent = tokens.reshape(2, NY, NEW * 32).transpose(1, 0, 2).reshape(NY, 1, 2, 128)
    sent = jnp.broadcast_to(sent, (NY, NX * NC, 2, 128)).reshape(32, 2, 128)
    got = exchange(sent, ("y", "x", "c")).reshape(NY, 64, 32)
    resid = got.transpose(1, 0, 2).reshape(64, 128)

    def over_heads(branch):
        return jnp.sum(to_all(branch.astype(BF16), ("x", "c")).astype(F32), axis=0)

    branch = over_heads(half(resid, gains[0], first[:, :1280], first[:, 1280:1920]))
    resid = (resid.astype(F32) + 0.5 * branch).astype(BF16)

    total, small = projected(resid, gains[1], rest[:, :1024], rest[:, 3200:])
    heads = total.reshape(NEW, 4, 2, HEAD_DIM)
    first_head = 2 * lax.axis_index(("x", "c"))
    mixed, state_out = advance(
        heads[:, 0],
        heads[:, 1],
        heads[:, 2],
        heads[:, 3],
        lax.dynamic_slice_in_dim(small, first_head, 2, 1),
        lax.dynamic_slice_in_dim(small, 16 + first_head, 2, 1),
        memory_state[0],
        lengths[0],
        decay_rate,
        decay_bias,
        head_gain,
    )
    mixed = to_all(mixed, "z").reshape(64, 256)
    branch = over_heads(
        lax.dot_general(
            mixed, rest[:, 1024:1280], (((1,), (1,)), ((), ())), preferred_element_type=F32
        )
    )
    resid = (resid.astype(F32) + branch).astype(BF16)

    branch = half(resid, gains[2], rest[:, 1280:2560], rest[:, 2560:3200])
    both = jnp.stack([branch.astype(BF16), resid])
    both = both.reshape(2, NX * NC, 8, NY, 32).transpose(3, 1, 0, 2, 4).reshape(32, 4, 128)
    got = exchange(both, ("y", "x", "c")).reshape(NY, NX * NC, 2, 8, 32)
    branch = jnp.sum(got[:, :, 0].astype(F32), axis=1)
    out = (got[:, 0, 1].astype(F32) + 0.5 * branch).astype(BF16)
    out = out.reshape(NY, 2, NEW, 32).transpose(1, 0, 2, 3).reshape(32, 32)
    return out, state_out[None]


def solution(mesh):
    fine = Mesh(mesh.devices.reshape(NZ, NY, NX, NC), ("z", "y", "x", "c"))
    kv, tp = ("z", "y"), ("x", "c")
    in_specs = (
        P(tp, kv),
        P(kv),
        P(kv, tp, None, None),
        P(kv),
        P(kv, tp),
        P(kv, tp),
        P(tp, kv),
        P(kv),
        P(kv, tp),
        P(kv, tp),
        P(kv, tp),
        P(kv, tp),
        P(kv, None),
        P(kv, None),
        P(tp),
        P(tp),
        P(),
        P(tp, kv),
        P(kv),
        P(kv, tp),
        P(kv, tp),
        P(tp, kv),
    )
    out_specs = (P(tp, kv), P(kv, tp, None, None))
    return jax.shard_map(
        on_device, mesh=fine, in_specs=in_specs, out_specs=out_specs, check_vma=False
    )
```

time: 232 us -> 208 us (0.90)
  blocking collectives: 60.9 us -> 87.2 us
  starting transfers between devices: 65 us -> 41.3 us
  local copies, waits for them, and re-layouts: 25.7 us -> 10.6 us
  waiting for transfers between devices: 70.2 us -> 60 us
    all_to_all x3 -> x5, blocking collectives: 60.9 us -> 87.2 us  [exchange(): return lax.all_to_all(x, axes, 0, 0, tiled=True)]
    all_to_all x9 -> x7, starting transfers between devices: 65 us -> 41.3 us  [exchange(): return lax.all_to_all(x, axes, 0, 0, tiled=True)]
    all_to_all x9 -> x7, waiting for transfers between devices: 70.2 us -> 60 us  [exchange(): return lax.all_to_all(x, axes, 0, 0, tiled=True)]
    unnamed x52 -> x42, local copies, waits for them, and re-layouts: 8.02 us -> 1.46 us
    reshape x43 -> x12, local copies, waits for them, and re-layouts: 8.46 us -> 2.58 us  [the longest x3 0.79 us: projected(): got = exchange(out.reshape(NZ, NEW, -1), 'z')]
  transfers between devices with their start and end apart: 9 -> 7, of which waited for: 8 -> 7; matrix products, arithmetic and copies ran while one was open for 4% -> 2% of each run, Pallas kernels for 0% -> 0%
where the time goes in v2:
time: 208 us; the launch traced here: 207 us
  blocking collectives  87.2 us (42%)
  waiting for transfers between devices  60 us (29%)
  starting transfers between devices  41.3 us (20%)
  local copies, waits for them, and re-layouts  10.6 us (5%)
  other arithmetic  4.32 us (2%)
    all_to_all x5, blocking collectives, exchange(): return lax.all_to_all(x, axes, 0, 0, tiled=True)  87.2 us
    all_to_all x7, waiting for transfers between devices, exchange(): return lax.all_to_all(x, axes, 0, 0, tiled=True)  60 us
    all_to_all x7, starting transfers between devices, exchange(): return lax.all_to_all(x, axes, 0, 0, tiled=True)  41.3 us
  transfers between devices with their start and end apart: 7, of which 7 were waited for; matrix products, arithmetic and copies ran while one was open for 2% of the time, Pallas kernels for 0%

profile of v2, /device:TPU:1, one launch (start us, length us, event | category | flops | bytes accessed | tf_op | source)
XLA Modules:
  0.0 206.6 jit_solution(13863076575802044425)
XLA Ops:
  0.6 0.8 reshape.378
  1.5 0.6 broadcast_in_dim.42
  2.1 10.4 %all-to-all-start = ((bf16[32,2,128]{2,1,0:T(2,128)(2,1)}), bf16[32,2,128]{2,1,0:T(2,128)(2,1)S(1)}, u32[]{:S(2)}, u32[]{:S(2)}) async-start(bf16[32,2,128]{2,1,0:T(2,128)(2,1)} %bitcast.1), calls=%async_computation | async-start | bytes 32768 | tf_op jit(solution)/shard_map/all_to_all | solution.py:17
  12.6 0.1 copy.154
  12.7 0.1 copy.155
  12.8 0.1 copy.156
  12.9 0.9 concatenate.24
  13.8 5.7 %all-to-all-done = bf16[32,2,128]{2,1,0:T(2,128)(2,1)S(1)} async-done(((bf16[32,2,128]{2,1,0:T(2,128)(2,1)}), bf16[32,2,128]{2,1,0:T(2,128)(2,1)S(1)}, u32[]{:S(2)}, u32[]{:S(2)}) %all-to-all-start) | async-done | bytes 16416 | tf_op jit(solution)/shard_map/all_to_all | solution.py:17
  19.6 0.8 broadcast_in_dim.43
  20.4 3.5 %all-to-all-start.1 = ((bf16[4,32,2048]{2,1,0:T(8,128)(2,1)}), bf16[4,32,2048]{2,1,0:T(8,128)(2,1)S(1)}, u32[]{:S(2)}, u32[]{:S(2)}) async-start(bf16[4,32,2048]{2,1,0:T(8,128)(2,1)} %broadcast_in_dim.43), calls=%async_computation.1 | async-start | bytes 1048576 | tf_op jit(solution)/shard_map/all_to_all | solution.py:17
  24.0 0.1 copy.153
  24.2 8.6 %all-to-all-done.1 = bf16[4,32,2048]{2,1,0:T(8,128)(2,1)S(1)} async-done(((bf16[4,32,2048]{2,1,0:T(8,128)(2,1)}), bf16[4,32,2048]{2,1,0:T(8,128)(2,1)S(1)}, u32[]{:S(2)}, u32[]{:S(2)}) %all-to-all-start.1) | async-done | bytes 524320 | tf_op jit(solution)/shard_map/all_to_all | solution.py:17
  32.9 0.3 convolution_convert_fusion.1
  33.3 25.1 %all_to_all.60 = bf16[16,4,1408]{2,1,0:T(4,128)(2,1)S(1)} all-to-all(bf16[16,4,1408]{2,1,0:T(4,128)(2,1)S(1)} %reshape.383), channel_id=1, replica_groups=mesh['z'=16,'y'=4,'x'=4,'c'=2] {'z'}, dimensions={0} | all-to-all | bytes 360448 | tf_op jit(solution)/shard_map/all_to_all | solution.py:17
  58.3 0.1 convert_reduce_fusion.1
  58.4 0.2 fusion.46
  58.7 19.0 %all_to_all.61 = bf16[16,4,640]{2,1,0:T(4,128)(2,1)S(1)} all-to-all(bf16[16,4,640]{2,1,0:T(4,128)(2,1)S(1)} %broadcast_in_dim.46), channel_id=1, replica_groups=mesh['z'=16,'y'=4,'x'=4,'c'=2] {'z'}, dimensions={0} | all-to-all | bytes 163840 | tf_op jit(solution)/shard_map/all_to_all | solution.py:17
  77.7 0.2 convolution_convert_fusion.5
  77.9 0.7 broadcast_in_dim.47
  78.7 6.5 %all-to-all-start.4 = ((bf16[8,64,128]{2,1,0:T(8,128)(2,1)}), bf16[8,64,128]{2,1,0:T(8,128)(2,1)S(1)}, u32[]{:S(2)}, u32[]{:S(2)}) async-start(bf16[8,64,128]{2,1,0:T(8,128)(2,1)} %broadcast_in_dim.47), calls=%async_computation.4 | async-start | bytes 262144 | tf_op jit(solution)/shard_map/all_to_all | solution.py:17
  85.2 0.1 copy.159
  85.3 0.1 copy.160
  85.5 0.5 copy-done.7
  86.0 0.1 concatenate.26
  86.1 4.4 %all-to-all-done.4 = bf16[8,64,128]{2,1,0:T(8,128)(2,1)S(1)} async-done(((bf16[8,64,128]{2,1,0:T(8,128)(2,1)}), bf16[8,64,128]{2,1,0:T(8,128)(2,1)S(1)}, u32[]{:S(2)}, u32[]{:S(2)}) %all-to-all-start.4) | async-done | bytes 131104 | tf_op jit(solution)/shard_map/all_to_all | solution.py:17
  90.5 1.0 broadcast_in_dim.48
  91.5 3.5 %all-to-all-start.5 = ((bf16[4,32,3328]{2,1,0:T(8,128)(2,1)}), bf16[4,32,3328]{2,1,0:T(8,128)(2,1)S(1)}, u32[]{:S(2)}, u32[]{:S(2)}) async-start(bf16[4,32,3328]{2,1,0:T(8,128)(2,1)} %broadcast_in_dim.48), calls=%async_computation.5 | async-start | bytes 1703936 | tf_op jit(solution)/shard_map/all_to_all | solution.py:17
  95.1 0.1 copy.161
  95.2 11.9 %all-to-all-done.5 = bf16[4,32,3328]{2,1,0:T(8,128)(2,1)S(1)} async-done(((bf16[4,32,3328]{2,1,0:T(8,128)(2,1)}), bf16[4,32,3328]{2,1,0:T(8,128)(2,1)S(1)}, u32[]{:S(2)}, u32[]{:S(2)}) %all-to-all-start.5) | async-done | bytes 852000 | tf_op jit(solution)/shard_map/all_to_all | solution.py:17
  107.2 0.2 convolution_convert_fusion.2
  107.5 0.7 reshape.386
  108.2 3.5 %all-to-all-start.6 = ((bf16[16,4,1152]{2,1,0:T(4,128)(2,1)}), bf16[16,4,1152]{2,1,0:T(4,128)(2,1)S(1)}, u32[]{:S(2)}, u32[]{:S(2)}) async-start(bf16[16,4,1152]{2,1,0:T(4,128)(2,1)} %reshape.386), calls=%async_computation.6 | async-start | bytes 294912 | tf_op jit(solution)/shard_map/all_to_all | solution.py:17
  112.4 11.3 %all-to-all-done.6 = bf16[16,4,1152]{2,1,0:T(4,128)(2,1)S(1)} async-done(((bf16[16,4,1152]{2,1,0:T(4,128)(2,1)}), bf16[16,4,1152]{2,1,0:T(4,128)(2,1)S(1)}, u32[]{:S(2)}, u32[]{:S(2)}) %all-to-all-start.6) | async-done | bytes 147488 | tf_op jit(solution)/shard_map/all_to_all | solution.py:17
  123.8 0.2 fusion.43
  124.2 0.1 multiply_reduce_fusion.10
  124.4 0.6 copy-done.17
  125.0 0.1 divide_multiply_fusion.6
  125.2 0.1 multiply_reduce_fusion.7
  125.3 0.2 multiply_reduce_fusion.6
  125.6 0.2 multiply_reduce_fusion.3
  125.9 0.2 multiply_reduce_fusion.2
  126.1 0.2 multiply_reduce_fusion.4
  126.4 0.2 fusion.32
  126.7 17.4 %all_to_all.62 = bf16[16,4,256]{2,1,0:T(4,128)(2,1)S(1)} all-to-all(bf16[16,4,256]{2,1,0:T(4,128)(2,1)S(1)} %broadcast_in_dim.50), channel_id=1, replica_groups=mesh['z'=16,'y'=4,'x'=4,'c'=2] {'z'}, dimensions={0} | all-to-all | bytes 65536 | tf_op jit(solution)/shard_map/all_to_all | solution.py:17
  144.1 0.1 convolution_convert_fusion.4
  144.3 10.8 %all_to_all.63 = bf16[8,64,128]{2,1,0:T(8,128)(2,1)S(1)} all-to-all(bf16[8,64,128]{2,1,0:T(8,128)(2,1)S(1)} %broadcast_in_dim.51), channel_id=1, replica_groups=mesh['z'=16,'y'=4,'x'=4,'c'=2] {'x','c'}, dimensions={0} | all-to-all | bytes 262144 | tf_op jit(solution)/shard_map/all_to_all | solution.py:17
  155.1 0.1 copy.164
  155.2 0.2 convolution_convert_fusion
  155.6 15.0 %all_to_all.64 = bf16[16,4,1408]{2,1,0:T(4,128)(2,1)S(1)} all-to-all(bf16[16,4,1408]{2,1,0:T(4,128)(2,1)S(1)} %reshape.389), channel_id=1, replica_groups=mesh['z'=16,'y'=4,'x'=4,'c'=2] {'z'}, dimensions={0} | all-to-all | bytes 360448 | tf_op jit(solution)/shard_map/all_to_all | solution.py:17
  170.6 0.1 convert_reduce_fusion
  170.7 0.2 fusion.40
  171.0 0.7 broadcast_in_dim.53
  171.6 8.1 %all-to-all-start.10 = ((bf16[16,4,640]{2,1,0:T(4,128)(2,1)}), bf16[16,4,640]{2,1,0:T(4,128)(2,1)S(1)}, u32[]{:S(2)}, u32[]{:S(2)}) async-start(bf16[16,4,640]{2,1,0:T(4,128)(2,1)} %broadcast_in_dim.53), calls=%async_computation.10 | async-start | bytes 163840 | tf_op jit(solution)/shard_map/all_to_all | solution.py:17
  179.7 0.1 mul.669
  179.8 0.1 reduce_sum.214
  180.0 11.5 %all-to-all-done.10 = bf16[16,4,640]{2,1,0:T(4,128)(2,1)S(1)} async-done(((bf16[16,4,640]{2,1,0:T(4,128)(2,1)}), bf16[16,4,640]{2,1,0:T(4,128)(2,1)S(1)}, u32[]{:S(2)}, u32[]{:S(2)}) %all-to-all-start.10) | async-done | bytes 81952 | tf_op jit(solution)/shard_map/all_to_all | solution.py:17
  191.6 0.2 convolution_convert_fusion.3
  191.8 0.1 stack.58
  192.0 0.7 reshape.391
  192.7 5.8 %all-to-all-start.11 = ((bf16[32,4,128]{2,1,0:T(4,128)(2,1)}), bf16[32,4,128]{2,1,0:T(4,128)(2,1)S(1)}, u32[]{:S(2)}, u32[]{:S(2)}) async-start(bf16[32,4,128]{2,1,0:T(4,128)(2,1)} %reshape.391), calls=%async_computation.11 | async-start | bytes 65536 | tf_op jit(solution)/shard_map/all_to_all | solution.py:17
  198.5 0.9 multiply_add_fusion
  199.4 6.5 %all-to-all-done.11 = bf16[32,4,128]{2,1,0:T(4,128)(2,1)S(1)} async-done(((bf16[32,4,128]{2,1,0:T(4,128)(2,1)}), bf16[32,4,128]{2,1,0:T(4,128)(2,1)S(1)}, u32[]{:S(2)}, u32[]{:S(2)}) %all-to-all-start.11) | async-done | bytes 32800 | tf_op jit(solution)/shard_map/all_to_all | solution.py:17
  205.9 0.1 reshape.392
  206.0 0.6 copy.171
  (101 shorter events, 2.3 us)
Async XLA Ops:
  0.6 111.8 %copy-start = (f32[128]{0:T(128)S(1)}, f32[128]{0:T(128)}, u32[]{:S(2)}) copy-start(f32[128]{0:T(128)} %param.38) | copy-start | bytes 1540
  1.4 11.1 %copy-start.14 = (f32[32]{0:T(128)S(1)}, f32[32]{0:T(128)}, u32[]{:S(2)}) copy-start(f32[32]{0:T(128)} %param.40) | copy-start | bytes 388
  1.4 11.1 %copy-start.15 = (f32[32]{0:T(128)S(1)}, f32[32]{0:T(128)}, u32[]{:S(2)}) copy-start(f32[32]{0:T(128)} %param.29) | copy-start | bytes 388
  1.4 11.1 %copy-start.16 = (f32[32]{0:T(128)S(1)}, f32[32]{0:T(128)}, u32[]{:S(2)}) copy-start(f32[32]{0:T(128)} %param.25) | copy-start | bytes 388
  1.5 11.4 %copy-start.3 = (bf16[32,640]{1,0:T(8,128)(2,1)S(1)}, bf16[32,640]{1,0:T(8,128)(2,1)}, u32[]{:S(2)}) copy-start(bf16[32,640]{1,0:T(8,128)(2,1)} %param.27) | copy-start | bytes 122884
  2.1 10.8 %copy-start.2 = (bf16[32,640]{1,0:T(8,128)(2,1)S(1)}, bf16[32,640]{1,0:T(8,128)(2,1)}, u32[]{:S(2)}) copy-start(bf16[32,640]{1,0:T(8,128)(2,1)} %param.26) | copy-start | bytes 122884
  2.1 17.5 %all-to-all-start = ((bf16[32,2,128]{2,1,0:T(2,128)(2,1)}), bf16[32,2,128]{2,1,0:T(2,128)(2,1)S(1)}, u32[]{:S(2)}, u32[]{:S(2)}) async-start(bf16[32,2,128]{2,1,0:T(2,128)(2,1)} %bitcast.1), calls=%async_computation | async-start | bytes 32768 | tf_op jit(solution)/shard_map/all_to_all | solution.py:17
  20.4 12.4 %all-to-all-start.1 = ((bf16[4,32,2048]{2,1,0:T(8,128)(2,1)}), bf16[4,32,2048]{2,1,0:T(8,128)(2,1)S(1)}, u32[]{:S(2)}, u32[]{:S(2)}) async-start(bf16[4,32,2048]{2,1,0:T(8,128)(2,1)} %broadcast_in_dim.43), calls=%async_computation.1 | async-start | bytes 1048576 | tf_op jit(solution)/shard_map/all_to_all | solution.py:17
  78.6 6.6 %copy-start.12 = (bf16[32,16]{0,1:T(8,128)(2,1)S(1)}, bf16[32,16]{0,1:T(8,128)(2,1)}, u32[]{:S(2)}) copy-start(bf16[32,16]{0,1:T(8,128)(2,1)} %param.34) | copy-start | bytes 3076
  78.6 6.7 %copy-start.13 = (bf16[32,16]{0,1:T(8,128)(2,1)S(1)}, bf16[32,16]{0,1:T(8,128)(2,1)}, u32[]{:S(2)}) copy-start(bf16[32,16]{0,1:T(8,128)(2,1)} %param.35) | copy-start | bytes 3076
  78.6 6.8 %copy-start.4 = (bf16[32,640]{1,0:T(8,128)(2,1)S(1)}, bf16[32,640]{1,0:T(8,128)(2,1)}, u32[]{:S(2)}) copy-start(bf16[32,640]{1,0:T(8,128)(2,1)} %param.41) | copy-start | bytes 122884
  78.6 6.8 %copy-start.5 = (bf16[32,640]{1,0:T(8,128)(2,1)S(1)}, bf16[32,640]{1,0:T(8,128)(2,1)}, u32[]{:S(2)}) copy-start(bf16[32,640]{1,0:T(8,128)(2,1)} %param.42) | copy-start | bytes 122884
  78.6 6.8 %copy-start.6 = (bf16[640,32]{0,1:T(8,128)(2,1)S(1)}, bf16[640,32]{0,1:T(8,128)(2,1)}, u32[]{:S(2)}) copy-start(bf16[640,32]{0,1:T(8,128)(2,1)} %param.43) | copy-start | bytes 122884
  78.6 6.8 %copy-start.8 = (bf16[32,256]{1,0:T(8,128)(2,1)S(1)}, bf16[32,256]{1,0:T(8,128)(2,1)}, u32[]{:S(2)}) copy-start(bf16[32,256]{1,0:T(8,128)(2,1)} %param.31) | copy-start | bytes 49156
  78.7 6.8 %copy-start.9 = (bf16[32,256]{1,0:T(8,128)(2,1)S(1)}, bf16[32,256]{1,0:T(8,128)(2,1)}, u32[]{:S(2)}) copy-start(bf16[32,256]{1,0:T(8,128)(2,1)} %param.32) | copy-start | bytes 49156
  78.7 6.8 %copy-start.10 = (bf16[32,256]{1,0:T(8,128)(2,1)S(1)}, bf16[32,256]{1,0:T(8,128)(2,1)}, u32[]{:S(2)}) copy-start(bf16[32,256]{1,0:T(8,128)(2,1)} %param.33) | copy-start | bytes 49156
  78.7 6.8 %copy-start.11 = (bf16[256,32]{0,1:T(8,128)(2,1)S(1)}, bf16[256,32]{0,1:T(8,128)(2,1)}, u32[]{:S(2)}) copy-start(bf16[256,32]{0,1:T(8,128)(2,1)} %param.39) | copy-start | bytes 49156
  78.7 11.8 %all-to-all-start.4 = ((bf16[8,64,128]{2,1,0:T(8,128)(2,1)}), bf16[8,64,128]{2,1,0:T(8,128)(2,1)S(1)}, u32[]{:S(2)}, u32[]{:S(2)}) async-start(bf16[8,64,128]{2,1,0:T(8,128)(2,1)} %broadcast_in_dim.47), calls=%async_computation.4 | async-start | bytes 262144 | tf_op jit(solution)/shard_map/all_to_all | solution.py:17
  85.2 0.7 copy-start.7
  91.5 15.7 %all-to-all-start.5 = ((bf16[4,32,3328]{2,1,0:T(8,128)(2,1)}), bf16[4,32,3328]{2,1,0:T(8,128)(2,1)S(1)}, u32[]{:S(2)}, u32[]{:S(2)}) async-start(bf16[4,32,3328]{2,1,0:T(8,128)(2,1)} %broadcast_in_dim.48), calls=%async_computation.5 | async-start | bytes 1703936 | tf_op jit(solution)/shard_map/all_to_all | solution.py:17
  108.2 15.5 %all-to-all-start.6 = ((bf16[16,4,1152]{2,1,0:T(4,128)(2,1)}), bf16[16,4,1152]{2,1,0:T(4,128)(2,1)S(1)}, u32[]{:S(2)}, u32[]{:S(2)}) async-start(bf16[16,4,1152]{2,1,0:T(4,128)(2,1)} %reshape.386), calls=%async_computation.6 | async-start | bytes 294912 | tf_op jit(solution)/shard_map/all_to_all | solution.py:17
  111.7 0.7 copy-start.18
  123.8 1.4 copy-start.1
  124.4 0.7 copy-start.17
  171.6 19.9 %all-to-all-start.10 = ((bf16[16,4,640]{2,1,0:T(4,128)(2,1)}), bf16[16,4,640]{2,1,0:T(4,128)(2,1)S(1)}, u32[]{:S(2)}, u32[]{:S(2)}) async-start(bf16[16,4,640]{2,1,0:T(4,128)(2,1)} %broadcast_in_dim.53), calls=%async_computation.10 | async-start | bytes 163840 | tf_op jit(solution)/shard_map/all_to_all | solution.py:17
  192.7 13.2 %all-to-all-start.11 = ((bf16[32,4,128]{2,1,0:T(4,128)(2,1)}), bf16[32,4,128]{2,1,0:T(4,128)(2,1)S(1)}, u32[]{:S(2)}, u32[]{:S(2)}) async-start(bf16[32,4,128]{2,1,0:T(4,128)(2,1)} %reshape.391), calls=%async_computation.11 | async-start | bytes 65536 | tf_op jit(solution)/shard_map/all_to_all | solution.py:17

commit v3 on v2

--- a/solution.py
+++ b/solution.py
@@ -31,12 +31,6 @@
     second = lax.reduce_precision(x - first, 8, 7)
     third = x - first - second
     return jnp.concatenate([first, second, third], axis=1).astype(BF16)
-
-
-def gather_weights(pieces):
-    own = jnp.concatenate(pieces, axis=1)
-    own = jnp.pad(own, ((0, 0), (0, -own.shape[1] % 128)))
-    return to_all(own, "y").reshape(128, -1)
 
 
 def projected(resid, gain, weight, tail):
@@ -111,36 +105,40 @@
     second_up,
     second_down,
 ):
+    weights = [
+        first_gate,
+        first_up,
+        first_down.T,
+        query_weight,
+        key_weight,
+        value_weight,
+        outgate_weight,
+        out_weight.T,
+        second_gate,
+        second_up,
+        second_down.T,
+    ]
     gains = jnp.stack([gain_first, gain_mixer, gain_second], axis=1)
-    first = gather_weights([first_gate, first_up, first_down.T, in_three(gains)])
-    rest = gather_weights(
-        [
-            query_weight,
-            key_weight,
-            value_weight,
-            outgate_weight,
-            out_weight.T,
-            second_gate,
-            second_up,
-            second_down.T,
-            beta_weight,
-            decay_weight,
-        ]
-    )
-    gains = jnp.sum(first[:, 1920:1929].astype(F32).T.reshape(3, 3, 128), axis=0)
-
-    sent = tokens.reshape(2, NY, NEW * 32).transpose(1, 0, 2).reshape(NY, 1, 2, 128)
-    sent = jnp.broadcast_to(sent, (NY, NX * NC, 2, 128)).reshape(32, 2, 128)
-    got = exchange(sent, ("y", "x", "c")).reshape(NY, 64, 32)
-    resid = got.transpose(1, 0, 2).reshape(64, 128)
+    tail = [beta_weight, decay_weight, in_three(gains), jnp.zeros((32, 75), BF16)]
+    own = jnp.concatenate([*weights, *tail], axis=1)
+    sent = tokens.T.reshape(32, 2, NY, NEW).transpose(2, 0, 1, 3).reshape(NY, 32, 8)
+    sent = jnp.pad(sent, ((0, 0), (0, 0), (0, 4)))
+    own = jnp.broadcast_to(own[None], (NY, *own.shape))
+    near = exchange(jnp.concatenate([own, sent], axis=2), "y").reshape(128, 5248)
+    w_up1, w_down1 = near[:, :1280], near[:, 1280:1920]
+    w_mix, w_out = near[:, 1920:2944], near[:, 2944:3200]
+    w_up2, w_down2 = near[:, 3200:4480], near[:, 4480:5120]
+    tail = near[:, 5120:]
+    gains = jnp.sum(tail[:, 32:41].astype(F32).T.reshape(3, 3, 128), axis=0)
+    resid = to_all(tail[:, 116:124].T, ("x", "c")).reshape(64, 128)
 
     def over_heads(branch):
         return jnp.sum(to_all(branch.astype(BF16), ("x", "c")).astype(F32), axis=0)
 
-    branch = over_heads(half(resid, gains[0], first[:, :1280], first[:, 1280:1920]))
+    branch = over_heads(half(resid, gains[0], w_up1, w_down1))
     resid = (resid.astype(F32) + 0.5 * branch).astype(BF16)
 
-    total, small = projected(resid, gains[1], rest[:, :1024], rest[:, 3200:])
+    total, small = projected(resid, gains[1], w_mix, tail)
     heads = total.reshape(NEW, 4, 2, HEAD_DIM)
     first_head = 2 * lax.axis_index(("x", "c"))
     mixed, state_out = advance(
@@ -158,13 +156,11 @@
     )
     mixed = to_all(mixed, "z").reshape(64, 256)
     branch = over_heads(
-        lax.dot_general(
-            mixed, rest[:, 1024:1280], (((1,), (1,)), ((), ())), preferred_element_type=F32
-        )
+        lax.dot_general(mixed, w_out, (((1,), (1,)), ((), ())), preferred_element_type=F32)
     )
     resid = (resid.astype(F32) + branch).astype(BF16)
 
-    branch = half(resid, gains[2], rest[:, 1280:2560], rest[:, 2560:3200])
+    branch = half(resid, gains[2], w_up2, w_down2)
     both = jnp.stack([branch.astype(BF16), resid])
     both = both.reshape(2, NX * NC, 8, NY, 32).transpose(3, 1, 0, 2, 4).reshape(32, 4, 128)
     got = exchange(both, ("y", "x", "c")).reshape(NY, NX * NC, 2, 8, 32)

time: 208 us -> 199 us (0.957)
  waiting for transfers between devices: 60 us -> 46.4 us
  blocking collectives: 87.2 us -> 100 us
  starting transfers between devices: 41.3 us -> 33.2 us
  other arithmetic: 4.32 us -> 6.53 us
    all_to_all x7 -> x5, waiting for transfers between devices: 60 us -> 46.4 us  [exchange(): return lax.all_to_all(x, axes, 0, 0, tiled=True)]
    all_to_all x5 -> x6, blocking collectives: 87.2 us -> 100 us  [exchange(): return lax.all_to_all(x, axes, 0, 0, tiled=True)]
    all_to_all x7 -> x5, starting transfers between devices: 41.3 us -> 33.2 us  [exchange(): return lax.all_to_all(x, axes, 0, 0, tiled=True)]
  transfers between devices with their start and end apart: 7 -> 5, of which waited for: 7 -> 5; matrix products, arithmetic and copies ran while one was open for 2% -> 1% of each run, Pallas kernels for 0% -> 0%
where the time goes in v3:
time: 199 us; the launch traced here: 198 us
  blocking collectives  100 us (50%)
  waiting for transfers between devices  46.4 us (23%)
  starting transfers between devices  33.2 us (17%)
  local copies, waits for them, and re-layouts  8.63 us (4%)
  other arithmetic  6.53 us (3%)
    all_to_all x6, blocking collectives, exchange(): return lax.all_to_all(x, axes, 0, 0, tiled=True)  100 us
    all_to_all x5, waiting for transfers between devices, exchange(): return lax.all_to_all(x, axes, 0, 0, tiled=True)  46.4 us
    all_to_all x5, starting transfers between devices, exchange(): return lax.all_to_all(x, axes, 0, 0, tiled=True)  33.2 us
  transfers between devices with their start and end apart: 5, of which 5 were waited for; matrix products, arithmetic and copies ran while one was open for 1% of the time, Pallas kernels for 0%

profile of v3, /device:TPU:1, one launch (start us, length us, event | category | flops | bytes accessed | tf_op | source)
XLA Modules:
  0.0 197.8 jit_solution(4518341403526337363)
XLA Ops:
  0.6 0.7 fusion.37
  1.4 0.1 copy.101
  1.5 0.1 copy.102
  1.6 0.1 copy.103
  1.7 0.8 copy.100
  2.4 0.8 copy.99
  3.2 0.7 copy.104
  3.9 0.1 copy.116
  4.0 1.1 concatenate.24
  5.1 0.1 broadcast_in_dim.49
  5.2 1.2 fusion.1
  6.3 5.0 %all-to-all-start = ((bf16[4,32,5248]{2,1,0:T(8,128)(2,1)}), bf16[4,32,5248]{2,1,0:T(8,128)(2,1)S(1)}, u32[]{:S(2)}, u32[]{:S(2)}) async-start(bf16[4,32,5248]{2,1,0:T(8,128)(2,1)} %fusion.1), calls=%async_computation | async-start | bytes 2686976 | tf_op jit(solution)/shard_map/all_to_all | solution.py:17
  11.4 12.7 %all-to-all-done = bf16[4,32,5248]{2,1,0:T(8,128)(2,1)S(1)} async-done(((bf16[4,32,5248]{2,1,0:T(8,128)(2,1)}), bf16[4,32,5248]{2,1,0:T(8,128)(2,1)S(1)}, u32[]{:S(2)}, u32[]{:S(2)}) %all-to-all-start) | async-done | bytes 1343520 | tf_op jit(solution)/shard_map/all_to_all | solution.py:17
  24.3 0.6 broadcast_in_dim.50
  24.9 10.8 %all-to-all-start.1 = ((bf16[8,8,128]{2,1,0:T(8,128)(2,1)}), bf16[8,8,128]{2,1,0:T(8,128)(2,1)S(1)}, u32[]{:S(2)}, u32[]{:S(2)}) async-start(bf16[8,8,128]{2,1,0:T(8,128)(2,1)} %broadcast_in_dim.50), calls=%async_computation.1 | async-start | bytes 32768 | tf_op jit(solution)/shard_map/all_to_all | solution.py:17
  35.8 4.5 %all-to-all-done.1 = bf16[8,8,128]{2,1,0:T(8,128)(2,1)S(1)} async-done(((bf16[8,8,128]{2,1,0:T(8,128)(2,1)}), bf16[8,8,128]{2,1,0:T(8,128)(2,1)S(1)}, u32[]{:S(2)}, u32[]{:S(2)}) %all-to-all-start.1) | async-done | bytes 16416 | tf_op jit(solution)/shard_map/all_to_all | solution.py:17
  40.4 0.1 fusion.17
  40.5 0.1 broadcast_in_dim.51
  40.6 0.2 convolution_convert_fusion.1
  40.9 27.0 %all_to_all.55 = bf16[16,4,1408]{2,1,0:T(4,128)(2,1)S(1)} all-to-all(bf16[16,4,1408]{2,1,0:T(4,128)(2,1)S(1)} %reshape.377), channel_id=1, replica_groups=mesh['z'=16,'y'=4,'x'=4,'c'=2] {'z'}, dimensions={0} | all-to-all | bytes 360448 | tf_op jit(solution)/shard_map/all_to_all | solution.py:17
  67.9 0.1 convert_reduce_fusion.1
  67.9 0.2 fusion.49
  68.3 20.0 %all_to_all.56 = bf16[16,4,640]{2,1,0:T(4,128)(2,1)S(1)} all-to-all(bf16[16,4,640]{2,1,0:T(4,128)(2,1)S(1)} %broadcast_in_dim.54), channel_id=1, replica_groups=mesh['z'=16,'y'=4,'x'=4,'c'=2] {'z'}, dimensions={0} | all-to-all | bytes 163840 | tf_op jit(solution)/shard_map/all_to_all | solution.py:17
  88.3 0.2 convolution_convert_fusion.5
  88.6 10.1 %all_to_all.57 = bf16[8,64,128]{2,1,0:T(8,128)(2,1)S(1)} all-to-all(bf16[8,64,128]{2,1,0:T(8,128)(2,1)S(1)} %broadcast_in_dim.55), channel_id=1, replica_groups=mesh['z'=16,'y'=4,'x'=4,'c'=2] {'x','c'}, dimensions={0} | all-to-all | bytes 262144 | tf_op jit(solution)/shard_map/all_to_all | solution.py:17
  98.7 0.1 fusion.11
  98.8 0.1 broadcast_in_dim.56
  98.9 0.2 convolution_convert_fusion.2
  99.3 0.7 reshape.379
  100.0 3.5 %all-to-all-start.5 = ((bf16[16,4,1152]{2,1,0:T(4,128)(2,1)}), bf16[16,4,1152]{2,1,0:T(4,128)(2,1)S(1)}, u32[]{:S(2)}, u32[]{:S(2)}) async-start(bf16[16,4,1152]{2,1,0:T(4,128)(2,1)} %reshape.379), calls=%async_computation.5 | async-start | bytes 294912 | tf_op jit(solution)/shard_map/all_to_all | solution.py:17
  104.2 11.3 %all-to-all-done.5 = bf16[16,4,1152]{2,1,0:T(4,128)(2,1)S(1)} async-done(((bf16[16,4,1152]{2,1,0:T(4,128)(2,1)}), bf16[16,4,1152]{2,1,0:T(4,128)(2,1)S(1)}, u32[]{:S(2)}, u32[]{:S(2)}) %all-to-all-start.5) | async-done | bytes 147488 | tf_op jit(solution)/shard_map/all_to_all | solution.py:17
  115.5 0.2 fusion.46
  115.9 0.1 multiply_reduce_fusion.10
  116.2 0.1 divide_multiply_fusion.6
  116.3 0.1 multiply_reduce_fusion.7
  116.5 0.2 multiply_reduce_fusion.6
  116.7 0.2 multiply_reduce_fusion.3
  117.0 0.2 multiply_reduce_fusion.2
  117.3 0.2 multiply_reduce_fusion.4
  117.5 0.2 fusion.35
  117.8 18.3 %all_to_all.58 = bf16[16,4,256]{2,1,0:T(4,128)(2,1)S(1)} all-to-all(bf16[16,4,256]{2,1,0:T(4,128)(2,1)S(1)} %broadcast_in_dim.102), channel_id=1, replica_groups=mesh['z'=16,'y'=4,'x'=4,'c'=2] {'z'}, dimensions={0} | all-to-all | bytes 65536 | tf_op jit(solution)/shard_map/all_to_all | solution.py:17
  136.2 0.1 convolution_convert_fusion.4
  136.4 9.8 %all_to_all.59 = bf16[8,64,128]{2,1,0:T(8,128)(2,1)S(1)} all-to-all(bf16[8,64,128]{2,1,0:T(8,128)(2,1)S(1)} %broadcast_in_dim.103), channel_id=1, replica_groups=mesh['z'=16,'y'=4,'x'=4,'c'=2] {'x','c'}, dimensions={0} | all-to-all | bytes 262144 | tf_op jit(solution)/shard_map/all_to_all | solution.py:17
  146.2 0.2 convolution_convert_fusion
  146.4 0.1 multiply_reduce_fusion.8
  146.5 0.1 broadcast_in_dim.104
  146.7 15.0 %all_to_all.60 = bf16[16,4,1408]{2,1,0:T(4,128)(2,1)S(1)} all-to-all(bf16[16,4,1408]{2,1,0:T(4,128)(2,1)S(1)} %reshape.382), channel_id=1, replica_groups=mesh['z'=16,'y'=4,'x'=4,'c'=2] {'z'}, dimensions={0} | all-to-all | bytes 360448 | tf_op jit(solution)/shard_map/all_to_all | solution.py:17
  161.7 0.1 convert_reduce_fusion
  161.8 0.2 fusion.43
  162.1 0.7 broadcast_in_dim.106
  162.8 8.1 %all-to-all-start.9 = ((bf16[16,4,640]{2,1,0:T(4,128)(2,1)}), bf16[16,4,640]{2,1,0:T(4,128)(2,1)S(1)}, u32[]{:S(2)}, u32[]{:S(2)}) async-start(bf16[16,4,640]{2,1,0:T(4,128)(2,1)} %broadcast_in_dim.106), calls=%async_computation.9 | async-start | bytes 163840 | tf_op jit(solution)/shard_map/all_to_all | solution.py:17
  170.8 0.1 reshape.390
  171.0 0.1 mul.669
  171.1 0.1 reduce_sum.214
  171.3 11.4 %all-to-all-done.9 = bf16[16,4,640]{2,1,0:T(4,128)(2,1)S(1)} async-done(((bf16[16,4,640]{2,1,0:T(4,128)(2,1)}), bf16[16,4,640]{2,1,0:T(4,128)(2,1)S(1)}, u32[]{:S(2)}, u32[]{:S(2)}) %all-to-all-start.9) | async-done | bytes 81952 | tf_op jit(solution)/shard_map/all_to_all | solution.py:17
  182.7 0.2 convolution_convert_fusion.3
  182.9 0.1 stack.58
  183.0 0.1 maximum_bitcast_fusion
  183.1 0.7 reshape.384
  183.9 5.8 %all-to-all-start.10 = ((bf16[32,4,128]{2,1,0:T(4,128)(2,1)}), bf16[32,4,128]{2,1,0:T(4,128)(2,1)S(1)}, u32[]{:S(2)}, u32[]{:S(2)}) async-start(bf16[32,4,128]{2,1,0:T(4,128)(2,1)} %reshape.384), calls=%async_computation.10 | async-start | bytes 65536 | tf_op jit(solution)/shard_map/all_to_all | solution.py:17
  189.7 0.9 multiply_add_fusion
  190.5 6.5 %all-to-all-done.10 = bf16[32,4,128]{2,1,0:T(4,128)(2,1)S(1)} async-done(((bf16[32,4,128]{2,1,0:T(4,128)(2,1)}), bf16[32,4,128]{2,1,0:T(4,128)(2,1)S(1)}, u32[]{:S(2)}, u32[]{:S(2)}) %all-to-all-start.10) | async-done | bytes 32800 | tf_op jit(solution)/shard_map/all_to_all | solution.py:17
  197.0 0.1 reshape.385
  197.2 0.6 copy.112
  (66 shorter events, 2.1 us)
Async XLA Ops:
  0.6 103.5 %copy-start = (f32[128]{0:T(128)S(1)}, f32[128]{0:T(128)}, u32[]{:S(2)}) copy-start(f32[128]{0:T(128)} %param.38) | copy-start | bytes 1540
  6.3 17.7 %all-to-all-start = ((bf16[4,32,5248]{2,1,0:T(8,128)(2,1)}), bf16[4,32,5248]{2,1,0:T(8,128)(2,1)S(1)}, u32[]{:S(2)}, u32[]{:S(2)}) async-start(bf16[4,32,5248]{2,1,0:T(8,128)(2,1)} %fusion.1), calls=%async_computation | async-start | bytes 2686976 | tf_op jit(solution)/shard_map/all_to_all | solution.py:17
  24.9 15.5 %all-to-all-start.1 = ((bf16[8,8,128]{2,1,0:T(8,128)(2,1)}), bf16[8,8,128]{2,1,0:T(8,128)(2,1)S(1)}, u32[]{:S(2)}, u32[]{:S(2)}) async-start(bf16[8,8,128]{2,1,0:T(8,128)(2,1)} %broadcast_in_dim.50), calls=%async_computation.1 | async-start | bytes 32768 | tf_op jit(solution)/shard_map/all_to_all | solution.py:17
  88.3 15.8 %copy-start.3 = (f32[2]{0:T(128)S(1)}, f32[2]{0:T(128)}, u32[]{:S(2)}) copy-start(f32[2]{0:T(128)} %param.36) | copy-start | bytes 28
  88.3 27.8 %copy-start.2 = (f32[2]{0:T(128)S(1)}, f32[2]{0:T(128)}, u32[]{:S(2)}) copy-start(f32[2]{0:T(128)} %param.37) | copy-start | bytes 28
  88.5 27.8 %copy-start.1 = (f32[1,2,128,128]{3,2,1,0:T(8,128)S(1)}, f32[1,2,128,128]{3,2,1,0:T(8,128)}, u32[]{:S(2)}) copy-start(f32[1,2,128,128]{3,2,1,0:T(8,128)} %param.24) | copy-start | bytes 393220
  100.0 15.5 %all-to-all-start.5 = ((bf16[16,4,1152]{2,1,0:T(4,128)(2,1)}), bf16[16,4,1152]{2,1,0:T(4,128)(2,1)S(1)}, u32[]{:S(2)}, u32[]{:S(2)}) async-start(bf16[16,4,1152]{2,1,0:T(4,128)(2,1)} %reshape.379), calls=%async_computation.5 | async-start | bytes 294912 | tf_op jit(solution)/shard_map/all_to_all | solution.py:17
  162.8 19.9 %all-to-all-start.9 = ((bf16[16,4,640]{2,1,0:T(4,128)(2,1)}), bf16[16,4,640]{2,1,0:T(4,128)(2,1)S(1)}, u32[]{:S(2)}, u32[]{:S(2)}) async-start(bf16[16,4,640]{2,1,0:T(4,128)(2,1)} %broadcast_in_dim.106), calls=%async_computation.9 | async-start | bytes 163840 | tf_op jit(solution)/shard_map/all_to_all | solution.py:17
  183.9 13.2 %all-to-all-start.10 = ((bf16[32,4,128]{2,1,0:T(4,128)(2,1)}), bf16[32,4,128]{2,1,0:T(4,128)(2,1)S(1)}, u32[]{:S(2)}, u32[]{:S(2)}) async-start(bf16[32,4,128]{2,1,0:T(4,128)(2,1)} %reshape.384), calls=%async_computation.10 | async-start | bytes 65536 | tf_op jit(solution)/shard_map/all_to_all | solution.py:17

commit v4 on v2

v4 whole, which is shorter than its diff:
```python
import jax
import jax.numpy as jnp
from jax import lax
from jax.experimental import pallas as pl
from jax.experimental.pallas import tpu as pltpu
from jax.sharding import Mesh, PartitionSpec as P

D = 2048
HEAD_DIM = 128
NEW = 4
EPS = 1e-06

NZ, NY, NX, NC = 16, 4, 4, 2
F32 = jnp.float32
BF16 = jnp.bfloat16


def exchange(x, axes):
    return lax.all_to_all(x, axes, 0, 0, tiled=True)


def to_all(x, axes):
    count = lax.axis_size(axes)
    return exchange(jnp.broadcast_to(x[None], (count, *x.shape)), axes)


def dot(a, b):
    return jnp.dot(a, b, preferred_element_type=F32)


def projected(resid, gain, weight, tail):
    wide = resid.astype(F32)
    squares = jnp.sum(wide * wide, axis=1, keepdims=True)
    operand = (wide * gain).astype(BF16)
    last = jnp.concatenate([dot(operand, tail)[:, :127], squares], axis=1)
    out = jnp.concatenate([dot(operand, weight).astype(BF16), last.astype(BF16)], axis=1)
    return exchange(out.reshape(NZ, NEW, -1), "z")


def summed(got):
    total = jnp.sum(got.astype(F32), axis=0)
    scale = lax.rsqrt(total[:, -1:] / D + EPS)
    return total[:, :-128] * scale, total[:, -128:] * scale


def half(resid, gain, w_up, w_down, tail):
    total, _ = summed(projected(resid, gain, w_up, tail))
    hidden = (jax.nn.silu(total[:, :640]) * total[:, 640:]).astype(BF16)
    hidden = to_all(hidden, "z").reshape(64, 640)
    return lax.dot_general(hidden, w_down, (((1,), (1,)), ((), ())), preferred_element_type=F32)


def advance(q, k, v, z, beta_logit, decay_logit, state_now, live, decay_rate, decay_bias, head_gain):
    query = jax.nn.silu(q)
    query = (
        query * lax.rsqrt(jnp.sum(query * query, axis=-1, keepdims=True) + EPS) * HEAD_DIM ** (-0.5)
    )
    keyvec = jax.nn.silu(k)
    keyvec = keyvec * lax.rsqrt(jnp.sum(keyvec * keyvec, axis=-1, keepdims=True) + EPS)
    values = jax.nn.silu(v)
    beta = jax.nn.sigmoid(beta_logit) * live
    decay = jnp.exp(-decay_rate * jax.nn.softplus(decay_logit + decay_bias) * live)
    outputs = []
    for t in range(NEW):
        state_now = state_now * decay[t][:, None, None]
        predicted = jnp.sum(keyvec[t][:, :, None] * state_now, axis=1)
        update = beta[t][:, None] * (values[t] - predicted)
        state_now = state_now + keyvec[t][:, :, None] * update[:, None, :]
        outputs.append(jnp.sum(query[t][:, :, None] * state_now, axis=1))
    mixed = jnp.stack(outputs, axis=0) * live[..., None]
    mixed = mixed * lax.rsqrt(jnp.mean(mixed * mixed, axis=-1, keepdims=True) + EPS) * head_gain
    mixed = mixed * jax.nn.silu(z)
    return mixed.reshape(NEW, -1).astype(BF16), state_now


def pack_kernel(*refs):
    length_ref, tokens_ref, *refs = refs
    gain_refs, logit_refs, weight_refs = refs[:3], refs[3:5], refs[5:-2]
    out_ref, live_ref = refs[-2:]
    slot = lax.broadcasted_iota(jnp.int32, (NEW, 128), 0)
    live_ref[...] = (slot < length_ref[0]).astype(F32)
    at = 0
    for ref in weight_refs:
        block = ref[...]
        for y in range(NY):
            out_ref[y, :, at : at + block.shape[1]] = block
        at += block.shape[1]
    gains = jnp.concatenate([ref[...] for ref in gain_refs], axis=0)
    first = gains.astype(BF16).astype(F32)
    second = (gains - first).astype(BF16).astype(F32)
    third = gains - first - second
    device = NC * lax.axis_index("x") + lax.axis_index("c")
    row = lax.broadcasted_iota(jnp.int32, (16, 32), 0)
    logits = []
    for ref in logit_refs:
        block = ref[...].astype(F32)
        for h in range(2):
            mine = jnp.where(row == 2 * device + h, block, 0.0)
            logits.append(jnp.sum(mine, axis=0, keepdims=True))
    gap = jnp.zeros((3, 32), F32)
    small = jnp.concatenate([*logits, first, second, third, gap], axis=0)
    rows = tokens_ref[...].astype(F32)
    end = jnp.zeros((104, 32), F32)
    for y in range(NY):
        mine = [rows[4 * y : 4 * y + 4], rows[16 + 4 * y : 20 + 4 * y]]
        tail = jnp.concatenate([small, *mine, end], axis=0)
        out_ref[y, :, at:] = tail.T.astype(BF16)


def pack(lengths, tokens, gains, logits, weights):
    gains = [g.reshape(1, 32) for g in gains]
    logits = [w.T for w in logits]
    space = pl.BlockSpec(memory_space=pltpu.VMEM)
    return pl.pallas_call(
        pack_kernel,
        out_shape=[
            jax.ShapeDtypeStruct((NY, 32, 5248), BF16),
            jax.ShapeDtypeStruct((NEW, 128), F32),
        ],
        in_specs=[pl.BlockSpec(memory_space=pltpu.SMEM)] + [space] * (6 + len(weights)),
        out_specs=[space, space],
        name="pack",
    )(lengths, tokens, *gains, *logits, *weights)


def on_device(
    tokens,
    lengths,
    memory_state,
    gain_first,
    first_gate,
    first_up,
    first_down,
    gain_mixer,
    query_weight,
    key_weight,
    value_weight,
    outgate_weight,
    beta_weight,
    decay_weight,
    decay_rate,
    decay_bias,
    head_gain,
    out_weight,
    gain_second,
    second_gate,
    second_up,
    second_down,
):
    near, live = pack(
        lengths,
        tokens,
        [gain_first, gain_mixer, gain_second],
        [beta_weight, decay_weight],
        [
            first_gate,
            first_up,
            first_down.T,
            query_weight,
            key_weight,
            value_weight,
            outgate_weight,
            out_weight.T,
            second_gate,
            second_up,
            second_down.T,
        ],
    )
    near = exchange(near, "y").reshape(128, 5248)
    w_up1, w_down1 = near[:, :1280], near[:, 1280:1920]
    w_mix, w_out = near[:, 1920:2944], near[:, 2944:3200]
    w_up2, w_down2 = near[:, 3200:4480], near[:, 4480:5120]
    tail = near[:, 5120:]
    got = to_all(tail[:, :32].T, ("x", "c"))
    resid = got[:, 16:24].reshape(64, 128)
    gains = jnp.sum(got[0, 4:13].astype(F32).reshape(3, 3, 128), axis=0)

    def over_heads(branch):
        return jnp.sum(to_all(branch.astype(BF16), ("x", "c")).astype(F32), axis=0)

    branch = over_heads(half(resid, gains[0], w_up1, w_down1, tail))
    resid = (resid.astype(F32) + 0.5 * branch).astype(BF16)

    got = projected(resid, gains[1], w_mix, tail)
    total, small = summed(got)
    heads = total.reshape(NEW, 4, 2, HEAD_DIM)
    mixed, state_out = advance(
        heads[:, 0],
        heads[:, 1],
        heads[:, 2],
        heads[:, 3],
        small[:, 0:2],
        small[:, 2:4],
        memory_state[0],
        live[:, :1],
        decay_rate,
        decay_bias,
        head_gain,
    )
    mixed, state_out = lax.optimization_barrier((mixed, state_out))
    mixed = to_all(mixed, "z").reshape(64, 256)
    branch = over_heads(
        lax.dot_general(mixed, w_out, (((1,), (1,)), ((), ())), preferred_element_type=F32)
    )
    resid = (resid.astype(F32) + branch).astype(BF16)

    branch = half(resid, gains[2], w_up2, w_down2, tail)
    branch, resid = lax.optimization_barrier((branch, resid))
    both = jnp.stack([branch.astype(BF16), resid])
    both = both.reshape(2, NX * NC, 8, NY, 32).transpose(3, 1, 0, 2, 4).reshape(32, 4, 128)
    got = exchange(both, ("y", "x", "c")).reshape(NY, NX * NC, 2, 8, 32)
    branch = jnp.sum(got[:, :, 0].astype(F32), axis=1)
    out = (got[:, 0, 1].astype(F32) + 0.5 * branch).astype(BF16)
    out = out.reshape(NY, 2, NEW, 32).transpose(1, 0, 2, 3).reshape(32, 32)
    return out, state_out[None]


def solution(mesh):
    fine = Mesh(mesh.devices.reshape(NZ, NY, NX, NC), ("z", "y", "x", "c"))
    kv, tp = ("z", "y"), ("x", "c")
    in_specs = (
        P(tp, kv),
        P(kv),
        P(kv, tp, None, None),
        P(kv),
        P(kv, tp),
        P(kv, tp),
        P(tp, kv),
        P(kv),
        P(kv, tp),
        P(kv, tp),
        P(kv, tp),
        P(kv, tp),
        P(kv, None),
        P(kv, None),
        P(tp),
        P(tp),
        P(),
        P(tp, kv),
        P(kv),
        P(kv, tp),
        P(kv, tp),
        P(tp, kv),
    )
    out_specs = (P(tp, kv), P(kv, tp, None, None))
    return jax.shard_map(
        on_device, mesh=fine, in_specs=in_specs, out_specs=out_specs, check_vma=False
    )
```

time: 208 us -> 194 us (0.933)
  blocking collectives: 87.2 us -> 166 us
  waiting for transfers between devices: 60 us -> 11.8 us
  starting transfers between devices: 41.3 us -> 3.51 us
  local copies, waits for them, and re-layouts: 10.6 us -> 3.02 us
  Pallas kernels: 0 us -> 2.19 us
    all_to_all x5 -> x10, blocking collectives: 87.2 us -> 166 us  [exchange(): return lax.all_to_all(x, axes, 0, 0, tiled=True)]
    all_to_all x7 -> x1, waiting for transfers between devices: 60 us -> 11.8 us  [exchange(): return lax.all_to_all(x, axes, 0, 0, tiled=True)]
    all_to_all x7 -> x1, starting transfers between devices: 41.3 us -> 3.51 us  [exchange(): return lax.all_to_all(x, axes, 0, 0, tiled=True)]
    broadcast_in_dim x7 -> x6, local copies, waits for them, and re-layouts: 3.25 us -> 0.2 us  [to_all(): return exchange(jnp.broadcast_to(x[None], (count, *x.shape)), axes)]
    pallas_call x0 -> x1, Pallas kernels: none -> 2.19 us  [pack(): pl.pallas_call(pack_kernel, out_shape=[jax.ShapeDtypeStruct((NY, 32, 5248...]
  transfers between devices with their start and end apart: 7 -> 1, of which waited for: 7 -> 1; matrix products, arithmetic and copies ran while one was open for 2% -> 0% of each run, Pallas kernels for 0% -> 0%
where the time goes in v4:
time: 194 us; the launch traced here: 193 us
  blocking collectives  166 us (86%)
  waiting for transfers between devices  11.8 us (6%)
  other arithmetic  4 us (2%)
  starting transfers between devices  3.51 us (2%)
  local copies, waits for them, and re-layouts  3.02 us (2%)
  Pallas kernels  2.19 us (1%)
    all_to_all x10, blocking collectives, exchange(): return lax.all_to_all(x, axes, 0, 0, tiled=True)  166 us
    all_to_all x1, waiting for transfers between devices, exchange(): return lax.all_to_all(x, axes, 0, 0, tiled=True)  11.8 us
  transfers between devices with their start and end apart: 1, of which 1 were waited for; matrix products, arithmetic and copies ran while one was open for 0% of the time, Pallas kernels for 0%

profile of v4, /device:TPU:1, one launch (start us, length us, event | category | flops | bytes accessed | tf_op | source)
XLA Modules:
  0.0 193.2 jit_solution(5615146495761794114)
XLA Ops:
  1.3 2.2 %pack.1 = (bf16[4,32,5248]{2,1,0:T(8,128)(2,1)}, f32[4,128]{1,0:T(4,128)}) custom-call(s32[1]{0:T(128)S(6)} %copy.98.refs_0_, bf16[32,32]{1,0:T(8,128)(2,1)} %refs_1_.1, f32[1,32]{1,0:T(1,128)} %bitcast.209, f32[1,32]{1,0:T(1,128)} %bitcast.210, f32[1,32]{1,0:T(1,128)} %bitcast.211, bf16[16,32]{1,0:T(8,128)(2,1)} %bitcast.207, bf16[16,32]{1,0:T(8,128)(2,1)} %bitcast.208, ...), custom_call_target="tpu_custom_call" | custom-call | tf_op jit(solution)/shard_map/pack/pallas_call | solution.py:114
  3.5 18.0 %all_to_all.55 = bf16[4,32,5248]{2,1,0:T(8,128)(2,1)S(1)} all-to-all(bf16[4,32,5248]{2,1,0:T(8,128)(2,1)} %get-tuple-element.8), channel_id=1, replica_groups=mesh['z'=16,'y'=4,'x'=4,'c'=2] {'y'}, dimensions={0} | all-to-all | bytes 2686976 | tf_op jit(solution)/shard_map/all_to_all | solution.py:19
  21.6 15.1 %all_to_all.56 = bf16[8,32,128]{2,1,0:T(8,128)(2,1)S(1)} all-to-all(bf16[8,32,128]{2,1,0:T(8,128)(2,1)S(1)} %broadcast_in_dim.23), channel_id=1, replica_groups=mesh['z'=16,'y'=4,'x'=4,'c'=2] {'x','c'}, dimensions={0} | all-to-all | bytes 131072 | tf_op jit(solution)/shard_map/all_to_all | solution.py:19
  36.8 0.1 fusion.15
  36.9 0.1 broadcast_in_dim.33
  37.0 0.1 fusion.21
  37.1 0.2 convolution_convert_fusion.1
  37.3 0.1 concatenate.20
  37.5 27.0 %all_to_all.57 = bf16[16,4,1408]{2,1,0:T(4,128)(2,1)S(1)} all-to-all(bf16[16,4,1408]{2,1,0:T(4,128)(2,1)S(1)} %reshape.223), channel_id=1, replica_groups=mesh['z'=16,'y'=4,'x'=4,'c'=2] {'z'}, dimensions={0} | all-to-all | bytes 360448 | tf_op jit(solution)/shard_map/all_to_all | solution.py:19
  64.4 0.1 convert_reduce_fusion.1
  64.5 0.2 fusion.53
  64.7 0.1 slice_multiply_fusion.1
  64.9 20.0 %all_to_all.58 = bf16[16,4,640]{2,1,0:T(4,128)(2,1)S(1)} all-to-all(bf16[16,4,640]{2,1,0:T(4,128)(2,1)S(1)} %broadcast_in_dim.25), channel_id=1, replica_groups=mesh['z'=16,'y'=4,'x'=4,'c'=2] {'z'}, dimensions={0} | all-to-all | bytes 163840 | tf_op jit(solution)/shard_map/all_to_all | solution.py:19
  85.0 0.2 convolution_convert_fusion.4
  85.2 10.0 %all_to_all.59 = bf16[8,64,128]{2,1,0:T(8,128)(2,1)S(1)} all-to-all(bf16[8,64,128]{2,1,0:T(8,128)(2,1)S(1)} %broadcast_in_dim.26), channel_id=1, replica_groups=mesh['z'=16,'y'=4,'x'=4,'c'=2] {'x','c'}, dimensions={0} | all-to-all | bytes 262144 | tf_op jit(solution)/shard_map/all_to_all | solution.py:19
  95.2 0.1 fusion.19
  95.3 0.2 convolution_convert_fusion.2
  95.5 0.1 fusion.11
  95.6 0.1 broadcast_in_dim.34
  95.7 0.1 concatenate.21
  95.8 0.7 reshape.225
  96.5 3.5 %all-to-all-start.5 = ((bf16[16,4,1152]{2,1,0:T(4,128)(2,1)}), bf16[16,4,1152]{2,1,0:T(4,128)(2,1)S(1)}, u32[]{:S(2)}, u32[]{:S(2)}) async-start(bf16[16,4,1152]{2,1,0:T(4,128)(2,1)} %reshape.225), calls=%async_computation.5 | async-start | bytes 294912 | tf_op jit(solution)/shard_map/all_to_all | solution.py:19
  100.1 0.1 slice_reduce_fusion
  100.2 11.8 %all-to-all-done.5 = bf16[16,4,1152]{2,1,0:T(4,128)(2,1)S(1)} async-done(((bf16[16,4,1152]{2,1,0:T(4,128)(2,1)}), bf16[16,4,1152]{2,1,0:T(4,128)(2,1)S(1)}, u32[]{:S(2)}, u32[]{:S(2)}) %all-to-all-start.5) | async-done | bytes 147488 | tf_op jit(solution)/shard_map/all_to_all | solution.py:19
  112.0 0.1 convert_reduce_fusion.2
  112.1 0.2 fusion.50
  112.3 0.1 slice_multiply_fusion.4
  112.4 0.1 slice_multiply_fusion.2
  112.5 0.1 multiply_reduce_fusion.9
  112.6 0.1 multiply_multiply_fusion
  112.7 0.1 divide_multiply_fusion.6
  112.8 0.1 multiply_reduce_fusion.7
  112.9 0.1 fusion.61
  113.0 0.2 multiply_reduce_fusion.6
  113.2 0.1 fusion.59
  113.3 0.2 multiply_reduce_fusion.3
  113.5 0.1 fusion.57
  113.5 0.2 multiply_reduce_fusion.2
  113.8 0.1 fusion.55
  113.8 0.8 multiply_reduce_fusion
  114.7 0.2 fusion.40
  114.8 0.1 broadcast_bitcast_fusion
  114.9 0.1 fusion.41
  115.0 18.3 %all_to_all.60 = bf16[16,4,256]{2,1,0:T(4,128)(2,1)S(1)} all-to-all(bf16[16,4,256]{2,1,0:T(4,128)(2,1)S(1)} %broadcast_in_dim.28), channel_id=1, replica_groups=mesh['z'=16,'y'=4,'x'=4,'c'=2] {'z'}, dimensions={0} | all-to-all | bytes 65536 | tf_op jit(solution)/shard_map/all_to_all | solution.py:19
  133.4 0.1 convolution_convert_fusion.3
  133.6 9.8 %all_to_all.61 = bf16[8,64,128]{2,1,0:T(8,128)(2,1)S(1)} all-to-all(bf16[8,64,128]{2,1,0:T(8,128)(2,1)S(1)} %broadcast_in_dim.29), channel_id=1, replica_groups=mesh['z'=16,'y'=4,'x'=4,'c'=2] {'x','c'}, dimensions={0} | all-to-all | bytes 262144 | tf_op jit(solution)/shard_map/all_to_all | solution.py:19
  143.4 0.1 fusion.17
  143.5 0.2 convolution_convert_fusion
  143.7 0.1 multiply_reduce_fusion.8
  143.8 0.1 broadcast_in_dim.35
  143.9 0.1 concatenate.22
  144.0 15.0 %all_to_all.62 = bf16[16,4,1408]{2,1,0:T(4,128)(2,1)S(1)} all-to-all(bf16[16,4,1408]{2,1,0:T(4,128)(2,1)S(1)} %reshape.228), channel_id=1, replica_groups=mesh['z'=16,'y'=4,'x'=4,'c'=2] {'z'}, dimensions={0} | all-to-all | bytes 360448 | tf_op jit(solution)/shard_map/all_to_all | solution.py:19
  159.0 0.1 convert_reduce_fusion
  159.1 0.2 fusion.47
  159.3 0.1 slice_multiply_fusion
  159.5 19.7 %all_to_all.63 = bf16[16,4,640]{2,1,0:T(4,128)(2,1)S(1)} all-to-all(bf16[16,4,640]{2,1,0:T(4,128)(2,1)S(1)} %broadcast_in_dim.31), channel_id=1, replica_groups=mesh['z'=16,'y'=4,'x'=4,'c'=2] {'z'}, dimensions={0} | all-to-all | bytes 163840 | tf_op jit(solution)/shard_map/all_to_all | solution.py:19
  179.2 0.2 fusion.3
  179.4 0.1 stack.44
  179.5 0.1 stack.45
  179.6 0.1 maximum_bitcast_fusion
  179.7 0.1 reshape.230
  179.9 12.5 %all_to_all.64 = bf16[32,4,128]{2,1,0:T(4,128)(2,1)S(1)} all-to-all(bf16[32,4,128]{2,1,0:T(4,128)(2,1)S(1)} %reshape.230), channel_id=1, replica_groups=mesh['z'=16,'y'=4,'x'=4,'c'=2] {'y','x','c'}, dimensions={0} | all-to-all | bytes 65536 | tf_op jit(solution)/shard_map/all_to_all | solution.py:19
  192.4 0.1 reshape.231
  192.6 0.6 copy.86
  (48 shorter events, 0.7 us)
Async XLA Ops:
  0.6 99.5 %copy-start = (f32[128]{0:T(128)S(1)}, f32[128]{0:T(128)}, u32[]{:S(2)}) copy-start(f32[128]{0:T(128)} %param.38) | copy-start | bytes 1540
  64.8 35.2 %copy-start.4 = (f32[2]{0:T(128)S(1)}, f32[2]{0:T(128)}, u32[]{:S(2)}) copy-start(f32[2]{0:T(128)} %param.36) | copy-start | bytes 28
  64.9 35.2 %copy-start.2 = (f32[4,128]{1,0:T(4,128)S(1)}, f32[4,128]{1,0:T(4,128)}, u32[]{:S(2)}) copy-start(f32[4,128]{1,0:T(4,128)} %get-tuple-element.9) | copy-start | bytes 6148
  84.9 27.8 %copy-start.3 = (f32[2]{0:T(128)S(1)}, f32[2]{0:T(128)}, u32[]{:S(2)}) copy-start(f32[2]{0:T(128)} %param.37) | copy-start | bytes 28
  84.9 27.9 %copy-start.1 = (f32[1,2,128,128]{3,2,1,0:T(8,128)S(1)}, f32[1,2,128,128]{3,2,1,0:T(8,128)}, u32[]{:S(2)}) copy-start(f32[1,2,128,128]{3,2,1,0:T(8,128)} %param.24) | copy-start | bytes 393220
  96.5 15.5 %all-to-all-start.5 = ((bf16[16,4,1152]{2,1,0:T(4,128)(2,1)}), bf16[16,4,1152]{2,1,0:T(4,128)(2,1)S(1)}, u32[]{:S(2)}, u32[]{:S(2)}) async-start(bf16[16,4,1152]{2,1,0:T(4,128)(2,1)} %reshape.225), calls=%async_computation.5 | async-start | bytes 294912 | tf_op jit(solution)/shard_map/all_to_all | solution.py:19

commit v5 on v4

--- a/solution.py
+++ b/solution.py
@@ -59,7 +59,7 @@
     keyvec = keyvec * lax.rsqrt(jnp.sum(keyvec * keyvec, axis=-1, keepdims=True) + EPS)
     values = jax.nn.silu(v)
     beta = jax.nn.sigmoid(beta_logit) * live
-    decay = jnp.exp(-decay_rate * jax.nn.softplus(decay_logit + decay_bias) * live)
+    decay = jnp.exp(decay_rate * jax.nn.softplus(decay_logit + decay_bias))
     outputs = []
     for t in range(NEW):
         state_now = state_now * decay[t][:, None, None]
@@ -67,18 +67,23 @@
         update = beta[t][:, None] * (values[t] - predicted)
         state_now = state_now + keyvec[t][:, :, None] * update[:, None, :]
         outputs.append(jnp.sum(query[t][:, :, None] * state_now, axis=1))
-    mixed = jnp.stack(outputs, axis=0) * live[..., None]
+    mixed = jnp.stack(outputs, axis=0) * live[:, :, None]
     mixed = mixed * lax.rsqrt(jnp.mean(mixed * mixed, axis=-1, keepdims=True) + EPS) * head_gain
     mixed = mixed * jax.nn.silu(z)
     return mixed.reshape(NEW, -1).astype(BF16), state_now
 
 
 def pack_kernel(*refs):
-    length_ref, tokens_ref, *refs = refs
-    gain_refs, logit_refs, weight_refs = refs[:3], refs[3:5], refs[5:-2]
-    out_ref, live_ref = refs[-2:]
-    slot = lax.broadcasted_iota(jnp.int32, (NEW, 128), 0)
-    live_ref[...] = (slot < length_ref[0]).astype(F32)
+    length_ref, rate_ref, bias_ref, head_gain_ref, tokens_ref, *refs = refs
+    gain_refs, logit_refs, weight_refs = refs[:3], refs[3:5], refs[5:-5]
+    out_ref, live_ref, minus_ref, wide_bias_ref, wide_gain_ref = refs[-5:]
+    slot = lax.broadcasted_iota(jnp.int32, (NEW, 2), 0)
+    live = (slot < jnp.broadcast_to(length_ref[...], (NEW, 2))).astype(F32)
+    live_ref[...] = live
+    minus_ref[...] = -rate_ref[...] * live
+    wide_bias_ref[...] = jnp.broadcast_to(bias_ref[...], (NEW, 2))
+    for t in range(NEW):
+        wide_gain_ref[t] = jnp.broadcast_to(head_gain_ref[...], (2, HEAD_DIM))
     at = 0
     for ref in weight_refs:
         block = ref[...]
@@ -107,7 +112,7 @@
         out_ref[y, :, at:] = tail.T.astype(BF16)
 
 
-def pack(lengths, tokens, gains, logits, weights):
+def pack(scalars, tokens, gains, logits, weights):
     gains = [g.reshape(1, 32) for g in gains]
     logits = [w.T for w in logits]
     space = pl.BlockSpec(memory_space=pltpu.VMEM)
@@ -115,12 +120,15 @@
         pack_kernel,
         out_shape=[
             jax.ShapeDtypeStruct((NY, 32, 5248), BF16),
-            jax.ShapeDtypeStruct((NEW, 128), F32),
+            jax.ShapeDtypeStruct((NEW, 2), F32),
+            jax.ShapeDtypeStruct((NEW, 2), F32),
+            jax.ShapeDtypeStruct((NEW, 2), F32),
+            jax.ShapeDtypeStruct((NEW, 2, HEAD_DIM), F32),
         ],
-        in_specs=[pl.BlockSpec(memory_space=pltpu.SMEM)] + [space] * (6 + len(weights)),
-        out_specs=[space, space],
+        in_specs=[space] * (10 + len(weights)),
+        out_specs=[space] * 5,
         name="pack",
-    )(lengths, tokens, *gains, *logits, *weights)
+    )(*(v.reshape(1, -1) for v in scalars), tokens, *gains, *logits, *weights)
 
 
 def on_device(
@@ -147,8 +155,8 @@
     second_up,
     second_down,
 ):
-    near, live = pack(
-        lengths,
+    near, live, rate, bias, wide_gain = pack(
+        [lengths, decay_rate, decay_bias, head_gain],
         tokens,
         [gain_first, gain_mixer, gain_second],
         [beta_weight, decay_weight],
@@ -192,10 +200,10 @@
         small[:, 0:2],
         small[:, 2:4],
         memory_state[0],
-        live[:, :1],
-        decay_rate,
-        decay_bias,
-        head_gain,
+        live,
+        rate,
+        bias,
+        wide_gain,
     )
     mixed, state_out = lax.optimization_barrier((mixed, state_out))
     mixed = to_all(mixed, "z").reshape(64, 256)

time: 194 us -> 192 us (0.990)
  blocking collectives: 166 us -> 180 us
  waiting for transfers between devices: 11.8 us -> 0 us
  starting transfers between devices: 3.51 us -> 0 us
    all_to_all x10 -> x11, blocking collectives: 166 us -> 180 us  [exchange(): return lax.all_to_all(x, axes, 0, 0, tiled=True)]
    all_to_all x1 -> x0, waiting for transfers between devices: 11.8 us -> none  [exchange(): return lax.all_to_all(x, axes, 0, 0, tiled=True)]
    all_to_all x1 -> x0, starting transfers between devices: 3.51 us -> none  [exchange(): return lax.all_to_all(x, axes, 0, 0, tiled=True)]
  transfers between devices with their start and end apart: 1 -> 0, of which waited for: 1 -> 0; matrix products, arithmetic and copies ran while one was open for 0% -> 0% of each run, Pallas kernels for 0% -> 0%
where the time goes in v5:
time: 192 us
  blocking collectives  180 us (94%)
  other arithmetic  4 us (2%)
  Pallas kernels  2.23 us (1%)
  local copies, waits for them, and re-layouts  2.17 us (1%)
    all_to_all x11, blocking collectives, exchange(): return lax.all_to_all(x, axes, 0, 0, tiled=True)  180 us

profile of v5, /device:TPU:1, one launch (start us, length us, event | category | flops | bytes accessed | tf_op | source)
XLA Modules:
  0.0 191.8 jit_solution(3673210472332469224)
XLA Ops:
  1.3 2.2 %pack.1 = (bf16[4,32,5248]{2,1,0:T(8,128)(2,1)}, f32[4,2]{1,0:T(4,128)}, f32[4,2]{1,0:T(4,128)}, f32[4,2]{1,0:T(4,128)}, f32[4,2,128]{2,1,0:T(2,128)}) custom-call(s32[1,1]{1,0:T(1,128)} %bitcast.170.refs_0_, f32[1,2]{1,0:T(1,128)} %bitcast.202, f32[1,2]{1,0:T(1,128)} %bitcast.203, f32[1,128]{1,0:T(1,128)} %bitcast.204, bf16[32,32]{1,0:T(8,128)(2,1)} %refs_4_.1, ...), custom_call_target="tpu_custom_call" | custom-call | tf_op jit(solution)/shard_map/pack/pallas_call | solution.py:119
  3.5 18.0 %all_to_all.55 = bf16[4,32,5248]{2,1,0:T(8,128)(2,1)S(1)} all-to-all(bf16[4,32,5248]{2,1,0:T(8,128)(2,1)} %get-tuple-element.11), channel_id=1, replica_groups=mesh['z'=16,'y'=4,'x'=4,'c'=2] {'y'}, dimensions={0} | all-to-all | bytes 2686976 | tf_op jit(solution)/shard_map/all_to_all | solution.py:19
  21.5 0.1 copy.49
  21.6 15.1 %all_to_all.56 = bf16[8,32,128]{2,1,0:T(8,128)(2,1)S(1)} all-to-all(bf16[8,32,128]{2,1,0:T(8,128)(2,1)S(1)} %broadcast_in_dim.23), channel_id=1, replica_groups=mesh['z'=16,'y'=4,'x'=4,'c'=2] {'x','c'}, dimensions={0} | all-to-all | bytes 131072 | tf_op jit(solution)/shard_map/all_to_all | solution.py:19
  36.8 0.1 fusion.15
  36.9 0.1 broadcast_in_dim.33
  37.0 0.1 fusion.21
  37.1 0.2 convolution_convert_fusion.1
  37.3 0.1 concatenate.19
  37.5 26.9 %all_to_all.57 = bf16[16,4,1408]{2,1,0:T(4,128)(2,1)S(1)} all-to-all(bf16[16,4,1408]{2,1,0:T(4,128)(2,1)S(1)} %reshape.226), channel_id=1, replica_groups=mesh['z'=16,'y'=4,'x'=4,'c'=2] {'z'}, dimensions={0} | all-to-all | bytes 360448 | tf_op jit(solution)/shard_map/all_to_all | solution.py:19
  64.4 0.1 convert_reduce_fusion.1
  64.5 0.2 fusion.47
  64.7 0.1 slice_multiply_fusion.1
  64.9 20.0 %all_to_all.58 = bf16[16,4,640]{2,1,0:T(4,128)(2,1)S(1)} all-to-all(bf16[16,4,640]{2,1,0:T(4,128)(2,1)S(1)} %broadcast_in_dim.25), channel_id=1, replica_groups=mesh['z'=16,'y'=4,'x'=4,'c'=2] {'z'}, dimensions={0} | all-to-all | bytes 163840 | tf_op jit(solution)/shard_map/all_to_all | solution.py:19
  84.9 0.0 copy-start.1
  85.0 0.0 copy-start
  85.0 0.2 convolution_convert_fusion.4
  85.1 0.1 broadcast_in_dim.26
  85.2 10.0 %all_to_all.59 = bf16[8,64,128]{2,1,0:T(8,128)(2,1)S(1)} all-to-all(bf16[8,64,128]{2,1,0:T(8,128)(2,1)S(1)} %broadcast_in_dim.26), channel_id=1, replica_groups=mesh['z'=16,'y'=4,'x'=4,'c'=2] {'x','c'}, dimensions={0} | all-to-all | bytes 262144 | tf_op jit(solution)/shard_map/all_to_all | solution.py:19
  95.2 0.1 fusion.19
  95.4 0.2 convolution_convert_fusion.2
  95.5 0.1 fusion.11
  95.6 0.1 broadcast_in_dim.34
  95.7 0.1 concatenate.20
  95.9 14.8 %all_to_all.60 = bf16[16,4,1152]{2,1,0:T(4,128)(2,1)S(1)} all-to-all(bf16[16,4,1152]{2,1,0:T(4,128)(2,1)S(1)} %reshape.228), channel_id=1, replica_groups=mesh['z'=16,'y'=4,'x'=4,'c'=2] {'z'}, dimensions={0} | all-to-all | bytes 294912 | tf_op jit(solution)/shard_map/all_to_all | solution.py:19
  110.6 0.1 convert_reduce_fusion.2
  110.7 0.2 fusion.44
  110.9 0.1 slice_multiply_fusion.4
  111.0 0.1 slice_multiply_fusion.2
  111.1 0.1 multiply_reduce_fusion.10
  111.2 0.1 multiply_multiply_fusion
  111.3 0.1 divide_multiply_fusion.6
  111.5 0.1 multiply_reduce_fusion.7
  111.6 0.1 fusion.56
  111.6 0.2 multiply_reduce_fusion.6
  111.8 0.1 fusion.54
  111.9 0.2 multiply_reduce_fusion.3
  112.1 0.1 fusion.52
  112.2 0.2 multiply_reduce_fusion.2
  112.4 0.1 fusion.50
  112.5 0.8 multiply_reduce_fusion
  113.3 0.2 multiply_reduce_fusion.9
  113.5 0.1 fusion.48
  113.6 17.7 %all_to_all.61 = bf16[16,4,256]{2,1,0:T(4,128)(2,1)S(1)} all-to-all(bf16[16,4,256]{2,1,0:T(4,128)(2,1)S(1)} %broadcast_in_dim.28), channel_id=1, replica_groups=mesh['z'=16,'y'=4,'x'=4,'c'=2] {'z'}, dimensions={0} | all-to-all | bytes 65536 | tf_op jit(solution)/shard_map/all_to_all | solution.py:19
  131.3 0.1 convolution_convert_fusion.3
  131.4 10.6 %all_to_all.62 = bf16[8,64,128]{2,1,0:T(8,128)(2,1)S(1)} all-to-all(bf16[8,64,128]{2,1,0:T(8,128)(2,1)S(1)} %broadcast_in_dim.29), channel_id=1, replica_groups=mesh['z'=16,'y'=4,'x'=4,'c'=2] {'x','c'}, dimensions={0} | all-to-all | bytes 262144 | tf_op jit(solution)/shard_map/all_to_all | solution.py:19
  142.1 0.1 fusion.17
  142.2 0.2 convolution_convert_fusion
  142.4 0.1 multiply_reduce_fusion.8
  142.5 0.1 broadcast_in_dim.35
  142.6 0.1 concatenate.21
  142.7 15.0 %all_to_all.63 = bf16[16,4,1408]{2,1,0:T(4,128)(2,1)S(1)} all-to-all(bf16[16,4,1408]{2,1,0:T(4,128)(2,1)S(1)} %reshape.231), channel_id=1, replica_groups=mesh['z'=16,'y'=4,'x'=4,'c'=2] {'z'}, dimensions={0} | all-to-all | bytes 360448 | tf_op jit(solution)/shard_map/all_to_all | solution.py:19
  157.7 0.1 convert_reduce_fusion
  157.8 0.2 fusion.41
  158.0 0.1 slice_multiply_fusion
  158.1 19.7 %all_to_all.64 = bf16[16,4,640]{2,1,0:T(4,128)(2,1)S(1)} all-to-all(bf16[16,4,640]{2,1,0:T(4,128)(2,1)S(1)} %broadcast_in_dim.31), channel_id=1, replica_groups=mesh['z'=16,'y'=4,'x'=4,'c'=2] {'z'}, dimensions={0} | all-to-all | bytes 163840 | tf_op jit(solution)/shard_map/all_to_all | solution.py:19
  177.9 0.2 fusion.3
  178.0 0.1 stack.29
  178.2 0.1 stack.30
  178.3 0.1 maximum_bitcast_fusion
  178.4 0.1 reshape.233
  178.5 12.5 %all_to_all.65 = bf16[32,4,128]{2,1,0:T(4,128)(2,1)S(1)} all-to-all(bf16[32,4,128]{2,1,0:T(4,128)(2,1)S(1)} %reshape.233), channel_id=1, replica_groups=mesh['z'=16,'y'=4,'x'=4,'c'=2] {'y','x','c'}, dimensions={0} | all-to-all | bytes 65536 | tf_op jit(solution)/shard_map/all_to_all | solution.py:19
  191.1 0.1 reshape.234
  191.2 0.6 copy.59
  (43 shorter events, 0.6 us)
Async XLA Ops:
  84.9 26.4 %copy-start.1 = (f32[4,2]{1,0:T(4,128)S(1)}, f32[4,2]{1,0:T(4,128)}, u32[]{:S(2)}) copy-start(f32[4,2]{1,0:T(4,128)} %get-tuple-element.14) | copy-start | bytes 100
  84.9 26.4 %copy-start.3 = (f32[4,2]{1,0:T(4,128)S(1)}, f32[4,2]{1,0:T(4,128)}, u32[]{:S(2)}) copy-start(f32[4,2]{1,0:T(4,128)} %get-tuple-element.12) | copy-start | bytes 100
  84.9 26.4 %copy-start.4 = (f32[4,2]{1,0:T(4,128)S(1)}, f32[4,2]{1,0:T(4,128)}, u32[]{:S(2)}) copy-start(f32[4,2]{1,0:T(4,128)} %get-tuple-element.13) | copy-start | bytes 100
  85.0 26.5 %copy-start = (f32[1,2,128,128]{3,2,1,0:T(8,128)S(1)}, f32[1,2,128,128]{3,2,1,0:T(8,128)}, u32[]{:S(2)}) copy-start(f32[1,2,128,128]{3,2,1,0:T(8,128)} %param.24) | copy-start | bytes 393220
  95.4 18.1 %copy-start.2 = (f32[4,2,128]{2,1,0:T(2,128)S(1)}, f32[4,2,128]{2,1,0:T(2,128)}, u32[]{:S(2)}) copy-start(f32[4,2,128]{2,1,0:T(2,128)} %get-tuple-element.15) | copy-start | bytes 12292

commit v6 on v5

--- a/solution.py
+++ b/solution.py
@@ -9,6 +9,7 @@
 HEAD_DIM = 128
 NEW = 4
 EPS = 1e-06
+
 
 NZ, NY, NX, NC = 16, 4, 4, 2
 F32 = jnp.float32
@@ -73,17 +74,17 @@
     return mixed.reshape(NEW, -1).astype(BF16), state_now
 
 
+def from_others(own):
+    blocks = [own]
+    for d in range(1, NY):
+        blocks.append(lax.ppermute(own, "y", [(y, y ^ d) for y in range(NY)]))
+    here = lax.axis_index("y")
+    return jnp.concatenate([lax.select_n(here ^ y, *blocks) for y in range(NY)], axis=0)
+
+
 def pack_kernel(*refs):
-    length_ref, rate_ref, bias_ref, head_gain_ref, tokens_ref, *refs = refs
-    gain_refs, logit_refs, weight_refs = refs[:3], refs[3:5], refs[5:-5]
-    out_ref, live_ref, minus_ref, wide_bias_ref, wide_gain_ref = refs[-5:]
-    slot = lax.broadcasted_iota(jnp.int32, (NEW, 2), 0)
-    live = (slot < jnp.broadcast_to(length_ref[...], (NEW, 2))).astype(F32)
-    live_ref[...] = live
-    minus_ref[...] = -rate_ref[...] * live
-    wide_bias_ref[...] = jnp.broadcast_to(bias_ref[...], (NEW, 2))
-    for t in range(NEW):
-        wide_gain_ref[t] = jnp.broadcast_to(head_gain_ref[...], (2, HEAD_DIM))
+    tokens_ref, *refs = refs
+    gain_refs, logit_refs, weight_refs, out_ref = refs[:3], refs[3:5], refs[5:-1], refs[-1]
     at = 0
     for ref in weight_refs:
         block = ref[...]
@@ -112,23 +113,50 @@
         out_ref[y, :, at:] = tail.T.astype(BF16)
 
 
-def pack(scalars, tokens, gains, logits, weights):
+def pack_far_kernel(length_ref, rate_ref, bias_ref, head_gain_ref, *refs):
+    weight_refs = refs[:-5]
+    far_ref, live_ref, minus_ref, wide_bias_ref, wide_gain_ref = refs[-5:]
+    slot = lax.broadcasted_iota(jnp.int32, (NEW, 2), 0)
+    live = (slot < jnp.broadcast_to(length_ref[...], (NEW, 2))).astype(F32)
+    live_ref[...] = live
+    minus_ref[...] = -rate_ref[...] * live
+    wide_bias_ref[...] = jnp.broadcast_to(bias_ref[...], (NEW, 2))
+    for t in range(NEW):
+        wide_gain_ref[t] = jnp.broadcast_to(head_gain_ref[...], (2, HEAD_DIM))
+    at = 0
+    for ref in weight_refs:
+        far_ref[:, at : at + ref.shape[1]] = ref[...]
+        at += ref.shape[1]
+
+
+def pack(tokens, gains, logits, weights):
     gains = [g.reshape(1, 32) for g in gains]
     logits = [w.T for w in logits]
     space = pl.BlockSpec(memory_space=pltpu.VMEM)
     return pl.pallas_call(
         pack_kernel,
+        out_shape=jax.ShapeDtypeStruct((NY, 32, 1408), BF16),
+        in_specs=[space] * (6 + len(weights)),
+        out_specs=space,
+        name="pack",
+    )(tokens, *gains, *logits, *weights)
+
+
+def pack_far(scalars, weights):
+    space = pl.BlockSpec(memory_space=pltpu.VMEM)
+    return pl.pallas_call(
+        pack_far_kernel,
         out_shape=[
-            jax.ShapeDtypeStruct((NY, 32, 5248), BF16),
+            jax.ShapeDtypeStruct((32, 3840), BF16),
             jax.ShapeDtypeStruct((NEW, 2), F32),
             jax.ShapeDtypeStruct((NEW, 2), F32),
             jax.ShapeDtypeStruct((NEW, 2), F32),
             jax.ShapeDtypeStruct((NEW, 2, HEAD_DIM), F32),
         ],
-        in_specs=[space] * (10 + len(weights)),
+        in_specs=[space] * (4 + len(weights)),
         out_specs=[space] * 5,
-        name="pack",
-    )(*(v.reshape(1, -1) for v in scalars), tokens, *gains, *logits, *weights)
+        name="pack_far",
+    )(*(v.reshape(1, -1) for v in scalars), *weights)
 
 
 def on_device(
@@ -155,14 +183,15 @@
     second_up,
     second_down,
 ):
-    near, live, rate, bias, wide_gain = pack(
-        [lengths, decay_rate, decay_bias, head_gain],
+    near = pack(
         tokens,
         [gain_first, gain_mixer, gain_second],
         [beta_weight, decay_weight],
+        [first_gate, first_up],
+    )
+    far, live, rate, bias, wide_gain = pack_far(
+        [lengths, decay_rate, decay_bias, head_gain],
         [
-            first_gate,
-            first_up,
             first_down.T,
             query_weight,
             key_weight,
@@ -174,11 +203,12 @@
             second_down.T,
         ],
     )
-    near = exchange(near, "y").reshape(128, 5248)
-    w_up1, w_down1 = near[:, :1280], near[:, 1280:1920]
-    w_mix, w_out = near[:, 1920:2944], near[:, 2944:3200]
-    w_up2, w_down2 = near[:, 3200:4480], near[:, 4480:5120]
-    tail = near[:, 5120:]
+    near = exchange(near, "y").reshape(128, 1408)
+    far = from_others(far)
+    w_up1, w_down1 = near[:, :1280], far[:, :640]
+    w_mix, w_out = far[:, 640:1664], far[:, 1664:1920]
+    w_up2, w_down2 = far[:, 1920:3200], far[:, 3200:]
+    tail = near[:, 1280:]
     got = to_all(tail[:, :32].T, ("x", "c"))
     resid = got[:, 16:24].reshape(64, 128)
     gains = jnp.sum(got[0, 4:13].astype(F32).reshape(3, 3, 128), axis=0)
@@ -186,7 +216,8 @@
     def over_heads(branch):
         return jnp.sum(to_all(branch.astype(BF16), ("x", "c")).astype(F32), axis=0)
 
-    branch = over_heads(half(resid, gains[0], w_up1, w_down1, tail))
+    branch = half(resid, gains[0], w_up1, w_down1, tail)
+    branch = over_heads(branch)
     resid = (resid.astype(F32) + 0.5 * branch).astype(BF16)
 
     got = projected(resid, gains[1], w_mix, tail)

time: 192 us -> 187 us (0.974)
  blocking collectives: 180 us -> 115 us
  starting transfers between devices: 0 us -> 39.3 us
  waiting for transfers between devices: 0 us -> 16.8 us
  local copies, waits for them, and re-layouts: 2.17 us -> 4.1 us
    all_to_all x11 -> x8, blocking collectives: 180 us -> 115 us  [exchange(): return lax.all_to_all(x, axes, 0, 0, tiled=True)]
    all_to_all x0 -> x3, starting transfers between devices: none -> 30.3 us  [exchange(): return lax.all_to_all(x, axes, 0, 0, tiled=True)]
    all_to_all x0 -> x3, waiting for transfers between devices: none -> 16.8 us  [exchange(): return lax.all_to_all(x, axes, 0, 0, tiled=True)]
    ppermute x0 -> x3, starting transfers between devices: none -> 8.97 us  [from_others(): blocks.append(lax.ppermute(own, 'y', [(y, y ^ d) for y in range(NY)]))]
  transfers between devices with their start and end apart: 0 -> 6, of which waited for: 0 -> 3; matrix products, arithmetic and copies ran while one was open for 0% -> 1% of each run, Pallas kernels for 0% -> 1%
where the time goes in v6:
time: 187 us
  blocking collectives  115 us (61%)
  starting transfers between devices  39.3 us (21%)
  waiting for transfers between devices  16.8 us (9%)
  other arithmetic  5.13 us (3%)
  local copies, waits for them, and re-layouts  4.1 us (2%)
  Pallas kernels  3.39 us (2%)
    all_to_all x8, blocking collectives, exchange(): return lax.all_to_all(x, axes, 0, 0, tiled=True)  115 us
    all_to_all x3, starting transfers between devices, exchange(): return lax.all_to_all(x, axes, 0, 0, tiled=True)  30.3 us
    all_to_all x3, waiting for transfers between devices, exchange(): return lax.all_to_all(x, axes, 0, 0, tiled=True)  16.8 us
    ppermute x3, starting transfers between devices, from_others(): blocks.append(lax.ppermute(own, 'y', [(y, y ^ d) for y in range(NY)]))  8.97 us
  transfers between devices with their start and end apart: 6, of which 3 were waited for; matrix products, arithmetic and copies ran while one was open for 1% of the time, Pallas kernels for 1%

profile of v6, /device:TPU:1, one launch (start us, length us, event | category | flops | bytes accessed | tf_op | source)
XLA Modules:
  0.0 186.5 jit_solution(9717319119980516802)
XLA Ops:
  0.6 1.7 pack.1
  2.4 11.1 %all_to_all.55 = bf16[4,32,1408]{2,1,0:T(8,128)(2,1)S(1)} all-to-all(bf16[4,32,1408]{2,1,0:T(8,128)(2,1)} %pack.1), channel_id=1, replica_groups=mesh['z'=16,'y'=4,'x'=4,'c'=2] {'y'}, dimensions={0} | all-to-all | bytes 720896 | tf_op jit(solution)/shard_map/all_to_all | solution.py:20
  13.5 13.6 %all_to_all.56 = bf16[8,32,128]{2,1,0:T(8,128)(2,1)S(1)} all-to-all(bf16[8,32,128]{2,1,0:T(8,128)(2,1)S(1)} %broadcast_in_dim.23), channel_id=1, replica_groups=mesh['z'=16,'y'=4,'x'=4,'c'=2] {'x','c'}, dimensions={0} | all-to-all | bytes 131072 | tf_op jit(solution)/shard_map/all_to_all | solution.py:20
  27.2 0.1 fusion.33
  27.3 0.1 broadcast_in_dim.33
  27.4 0.1 fusion.39
  27.5 0.2 convolution_convert_fusion.1
  27.7 0.1 concatenate.22
  27.8 0.7 reshape.222
  28.5 12.8 %all-to-all-start.2 = ((bf16[16,4,1408]{2,1,0:T(4,128)(2,1)}), bf16[16,4,1408]{2,1,0:T(4,128)(2,1)S(1)}, u32[]{:S(2)}, u32[]{:S(2)}) async-start(bf16[16,4,1408]{2,1,0:T(4,128)(2,1)} %reshape.222), calls=%async_computation.2 | async-start | bytes 360448 | tf_op jit(solution)/shard_map/all_to_all | solution.py:20
  42.0 1.7 pack_far.1
  43.7 2.8 %collective-permute-start.2 = (bf16[32,3840]{1,0:T(8,128)(2,1)}, bf16[32,3840]{1,0:T(8,128)(2,1)S(1)}, u32[]{:S(2)}, u32[]{:S(2)}) collective-permute-start(bf16[32,3840]{1,0:T(8,128)(2,1)} %get-tuple-element.11), channel_id=1, source_target_pairs={{0,24},{8,16},{16,8},{24,0},{1,25},{9,17},{17,9},{25,1},{2,26},{10... | collective-permute-start | bytes 737288 | tf_op jit(solution)/shard_map/ppermute | solution.py:80
  46.5 3.1 %collective-permute-start.1 = (bf16[32,3840]{1,0:T(8,128)(2,1)}, bf16[32,3840]{1,0:T(8,128)(2,1)S(1)}, u32[]{:S(2)}, u32[]{:S(2)}) collective-permute-start(bf16[32,3840]{1,0:T(8,128)(2,1)} %get-tuple-element.11), channel_id=1, source_target_pairs={{0,16},{8,24},{16,0},{24,8},{1,17},{9,25},{17,1},{25,9},{2,18},{10... | collective-permute-start | bytes 737288 | tf_op jit(solution)/shard_map/ppermute | solution.py:80
  49.6 3.1 %collective-permute-start = (bf16[32,3840]{1,0:T(8,128)(2,1)}, bf16[32,3840]{1,0:T(8,128)(2,1)S(1)}, u32[]{:S(2)}, u32[]{:S(2)}) collective-permute-start(bf16[32,3840]{1,0:T(8,128)(2,1)} %get-tuple-element.11), channel_id=1, source_target_pairs={{0,8},{8,0},{16,24},{24,16},{1,9},{9,1},{17,25},{25,17},{2,10},{10... | collective-permute-start | bytes 737288 | tf_op jit(solution)/shard_map/ppermute | solution.py:80
  52.7 0.9 all-to-all-done.2
  53.6 0.1 convert_reduce_fusion.1
  53.7 0.2 fusion.65
  53.9 0.1 slice_multiply_fusion.1
  54.0 0.7 broadcast_in_dim.25
  54.7 10.6 %all-to-all-start.3 = ((bf16[16,4,640]{2,1,0:T(4,128)(2,1)}), bf16[16,4,640]{2,1,0:T(4,128)(2,1)S(1)}, u32[]{:S(2)}, u32[]{:S(2)}) async-start(bf16[16,4,640]{2,1,0:T(4,128)(2,1)} %broadcast_in_dim.25), calls=%async_computation.3 | async-start | bytes 163840 | tf_op jit(solution)/shard_map/all_to_all | solution.py:20
  65.3 1.1 select_select_fusion.3
  66.3 10.8 %all-to-all-done.3 = bf16[16,4,640]{2,1,0:T(4,128)(2,1)S(1)} async-done(((bf16[16,4,640]{2,1,0:T(4,128)(2,1)}), bf16[16,4,640]{2,1,0:T(4,128)(2,1)S(1)}, u32[]{:S(2)}, u32[]{:S(2)}) %all-to-all-start.3) | async-done | bytes 81952 | tf_op jit(solution)/shard_map/all_to_all | solution.py:20
  77.1 0.2 convolution_convert_fusion.4
  77.3 0.7 broadcast_in_dim.26
  78.0 6.9 %all-to-all-start.4 = ((bf16[8,64,128]{2,1,0:T(8,128)(2,1)}), bf16[8,64,128]{2,1,0:T(8,128)(2,1)S(1)}, u32[]{:S(2)}, u32[]{:S(2)}) async-start(bf16[8,64,128]{2,1,0:T(8,128)(2,1)} %broadcast_in_dim.26), calls=%async_computation.4 | async-start | bytes 262144 | tf_op jit(solution)/shard_map/all_to_all | solution.py:20
  85.0 5.2 %all-to-all-done.4 = bf16[8,64,128]{2,1,0:T(8,128)(2,1)S(1)} async-done(((bf16[8,64,128]{2,1,0:T(8,128)(2,1)}), bf16[8,64,128]{2,1,0:T(8,128)(2,1)S(1)}, u32[]{:S(2)}, u32[]{:S(2)}) %all-to-all-start.4) | async-done | bytes 131104 | tf_op jit(solution)/shard_map/all_to_all | solution.py:20
  90.2 0.1 fusion.29
  90.3 0.1 broadcast_in_dim.34
  90.4 0.1 fusion.37
  90.5 0.2 convolution_convert_fusion.2
  90.7 0.1 concatenate.24
  90.9 14.6 %all_to_all.57 = bf16[16,4,1152]{2,1,0:T(4,128)(2,1)S(1)} all-to-all(bf16[16,4,1152]{2,1,0:T(4,128)(2,1)S(1)} %reshape.228), channel_id=1, replica_groups=mesh['z'=16,'y'=4,'x'=4,'c'=2] {'z'}, dimensions={0} | all-to-all | bytes 294912 | tf_op jit(solution)/shard_map/all_to_all | solution.py:20
  105.6 0.2 fusion.62
  105.9 0.1 multiply_reduce_fusion.10
  106.1 0.1 multiply_multiply_fusion
  106.2 0.1 divide_multiply_fusion.6
  106.3 0.1 multiply_reduce_fusion.7
  106.5 0.2 multiply_reduce_fusion.6
  106.7 0.2 multiply_reduce_fusion.3
  107.0 0.2 multiply_reduce_fusion.2
  107.3 0.8 multiply_reduce_fusion
  108.1 0.2 multiply_reduce_fusion.9
  108.3 0.1 fusion.66
  108.4 17.7 %all_to_all.58 = bf16[16,4,256]{2,1,0:T(4,128)(2,1)S(1)} all-to-all(bf16[16,4,256]{2,1,0:T(4,128)(2,1)S(1)} %broadcast_in_dim.28), channel_id=1, replica_groups=mesh['z'=16,'y'=4,'x'=4,'c'=2] {'z'}, dimensions={0} | all-to-all | bytes 65536 | tf_op jit(solution)/shard_map/all_to_all | solution.py:20
  126.1 0.1 convolution_convert_fusion.3
  126.3 10.4 %all_to_all.59 = bf16[8,64,128]{2,1,0:T(8,128)(2,1)S(1)} all-to-all(bf16[8,64,128]{2,1,0:T(8,128)(2,1)S(1)} %broadcast_in_dim.29), channel_id=1, replica_groups=mesh['z'=16,'y'=4,'x'=4,'c'=2] {'x','c'}, dimensions={0} | all-to-all | bytes 262144 | tf_op jit(solution)/shard_map/all_to_all | solution.py:20
  136.7 0.2 convolution_convert_fusion
  136.9 0.1 fusion.35
  137.0 0.1 multiply_reduce_fusion.8
  137.1 0.1 broadcast_in_dim.35
  137.2 0.1 concatenate.25
  137.4 15.0 %all_to_all.60 = bf16[16,4,1408]{2,1,0:T(4,128)(2,1)S(1)} all-to-all(bf16[16,4,1408]{2,1,0:T(4,128)(2,1)S(1)} %reshape.231), channel_id=1, replica_groups=mesh['z'=16,'y'=4,'x'=4,'c'=2] {'z'}, dimensions={0} | all-to-all | bytes 360448 | tf_op jit(solution)/shard_map/all_to_all | solution.py:20
  152.4 0.1 convert_reduce_fusion
  152.5 0.2 fusion.59
  152.7 0.1 slice_multiply_fusion
  152.8 19.7 %all_to_all.61 = bf16[16,4,640]{2,1,0:T(4,128)(2,1)S(1)} all-to-all(bf16[16,4,640]{2,1,0:T(4,128)(2,1)S(1)} %broadcast_in_dim.31), channel_id=1, replica_groups=mesh['z'=16,'y'=4,'x'=4,'c'=2] {'z'}, dimensions={0} | all-to-all | bytes 163840 | tf_op jit(solution)/shard_map/all_to_all | solution.py:20
  172.5 0.2 fusion.3
  172.7 0.1 stack.29
  172.8 0.1 stack.30
  172.9 0.1 maximum_bitcast_fusion
  173.1 0.1 reshape.233
  173.2 12.5 %all_to_all.62 = bf16[32,4,128]{2,1,0:T(4,128)(2,1)S(1)} all-to-all(bf16[32,4,128]{2,1,0:T(4,128)(2,1)S(1)} %reshape.233), channel_id=1, replica_groups=mesh['z'=16,'y'=4,'x'=4,'c'=2] {'y','x','c'}, dimensions={0} | all-to-all | bytes 65536 | tf_op jit(solution)/shard_map/all_to_all | solution.py:20
  185.7 0.1 reshape.234
  185.9 0.6 copy.59
  (55 shorter events, 1.2 us)
Async XLA Ops:
  28.5 25.1 %all-to-all-start.2 = ((bf16[16,4,1408]{2,1,0:T(4,128)(2,1)}), bf16[16,4,1408]{2,1,0:T(4,128)(2,1)S(1)}, u32[]{:S(2)}, u32[]{:S(2)}) async-start(bf16[16,4,1408]{2,1,0:T(4,128)(2,1)} %reshape.222), calls=%async_computation.2 | async-start | bytes 360448 | tf_op jit(solution)/shard_map/all_to_all | solution.py:20
  43.7 21.6 %collective-permute-start.2 = (bf16[32,3840]{1,0:T(8,128)(2,1)}, bf16[32,3840]{1,0:T(8,128)(2,1)S(1)}, u32[]{:S(2)}, u32[]{:S(2)}) collective-permute-start(bf16[32,3840]{1,0:T(8,128)(2,1)} %get-tuple-element.11), channel_id=1, source_target_pairs={{0,24},{8,16},{16,8},{24,0},{1,25},{9,17},{17,9},{25,1},{2,26},{10... | collective-permute-start | bytes 737288 | tf_op jit(solution)/shard_map/ppermute | solution.py:80
  46.5 18.8 %collective-permute-start.1 = (bf16[32,3840]{1,0:T(8,128)(2,1)}, bf16[32,3840]{1,0:T(8,128)(2,1)S(1)}, u32[]{:S(2)}, u32[]{:S(2)}) collective-permute-start(bf16[32,3840]{1,0:T(8,128)(2,1)} %get-tuple-element.11), channel_id=1, source_target_pairs={{0,16},{8,24},{16,0},{24,8},{1,17},{9,25},{17,1},{25,9},{2,18},{10... | collective-permute-start | bytes 737288 | tf_op jit(solution)/shard_map/ppermute | solution.py:80
  49.6 15.7 %collective-permute-start = (bf16[32,3840]{1,0:T(8,128)(2,1)}, bf16[32,3840]{1,0:T(8,128)(2,1)S(1)}, u32[]{:S(2)}, u32[]{:S(2)}) collective-permute-start(bf16[32,3840]{1,0:T(8,128)(2,1)} %get-tuple-element.11), channel_id=1, source_target_pairs={{0,8},{8,0},{16,24},{24,16},{1,9},{9,1},{17,25},{25,17},{2,10},{10... | collective-permute-start | bytes 737288 | tf_op jit(solution)/shard_map/ppermute | solution.py:80
  54.7 22.5 %all-to-all-start.3 = ((bf16[16,4,640]{2,1,0:T(4,128)(2,1)}), bf16[16,4,640]{2,1,0:T(4,128)(2,1)S(1)}, u32[]{:S(2)}, u32[]{:S(2)}) async-start(bf16[16,4,640]{2,1,0:T(4,128)(2,1)} %broadcast_in_dim.25), calls=%async_computation.3 | async-start | bytes 163840 | tf_op jit(solution)/shard_map/all_to_all | solution.py:20
  78.0 12.1 %all-to-all-start.4 = ((bf16[8,64,128]{2,1,0:T(8,128)(2,1)}), bf16[8,64,128]{2,1,0:T(8,128)(2,1)S(1)}, u32[]{:S(2)}, u32[]{:S(2)}) async-start(bf16[8,64,128]{2,1,0:T(8,128)(2,1)} %broadcast_in_dim.26), calls=%async_computation.4 | async-start | bytes 262144 | tf_op jit(solution)/shard_map/all_to_all | solution.py:20
  85.0 21.2 %copy-start.1 = (f32[4,2]{1,0:T(4,128)S(1)}, f32[4,2]{1,0:T(4,128)}, u32[]{:S(2)}) copy-start(f32[4,2]{1,0:T(4,128)} %get-tuple-element.14) | copy-start | bytes 100
  85.0 21.2 %copy-start.3 = (f32[4,2]{1,0:T(4,128)S(1)}, f32[4,2]{1,0:T(4,128)}, u32[]{:S(2)}) copy-start(f32[4,2]{1,0:T(4,128)} %get-tuple-element.12) | copy-start | bytes 100
  85.0 21.2 %copy-start.4 = (f32[4,2]{1,0:T(4,128)S(1)}, f32[4,2]{1,0:T(4,128)}, u32[]{:S(2)}) copy-start(f32[4,2]{1,0:T(4,128)} %get-tuple-element.13) | copy-start | bytes 100
  85.0 21.3 %copy-start = (f32[1,2,128,128]{3,2,1,0:T(8,128)S(1)}, f32[1,2,128,128]{3,2,1,0:T(8,128)}, u32[]{:S(2)}) copy-start(f32[1,2,128,128]{3,2,1,0:T(8,128)} %param.24) | copy-start | bytes 393220
  90.8 17.5 %copy-start.2 = (f32[4,2,128]{2,1,0:T(2,128)S(1)}, f32[4,2,128]{2,1,0:T(2,128)}, u32[]{:S(2)}) copy-start(f32[4,2,128]{2,1,0:T(2,128)} %get-tuple-element.15) | copy-start | bytes 12292
